TPU v7x, 32 devices: a whole 2x2x4 slice. The times are simulated.
32 devices in a mesh: sp: 8 (over z, x), tp: 4 (over y, core).
Axes of the slice: x: 2, y: 2, z: 4, core: 2. Of those that a mesh axis runs over, the one named last changes fastest.
Arguments:
- hidden_in: bfloat16 [3072, 2048], P('sp', 'tp'), may hold values from -6 to 6
- in_gain: float32 [2048], replicated, may hold values from 0.1 to 1.9
- receptance_weight: bfloat16 [2048, 1024], P(None, 'tp'), may hold values from -0.125 to 0.125
- key_weight: bfloat16 [2048, 1024], P(None, 'tp'), may hold values from -0.125 to 0.125
- value_weight: bfloat16 [2048, 1024], P(None, 'tp'), may hold values from -0.125 to 0.125
- decay_down: bfloat16 [2048, 128], replicated, may hold values from -0.125 to 0.125
- decay_up: bfloat16 [128, 1024], P(None, 'tp'), may hold values from -0.5 to 0.5
- decay_base: float32 [1024], P('tp'), may hold values from -14 to -2
- decay_shift: float32 [3072, 1024], P('sp', 'tp'), may hold values from -1 to 0
- learn_rate: float32 [1024], P('tp'), may hold values from 0 to 1
- query_pair: bfloat16 [2048, 8, 128], P(None, 'tp'), may hold values from -1 to 1
- key_pair: bfloat16 [2048, 8, 128], P(None, 'tp'), may hold values from -1 to 1
- value_pair: bfloat16 [2048, 8, 128], P(None, 'tp'), may hold values from -0.125 to 0.125
- mix_lambda: float32 [8], P('tp'), may hold values from 0.3 to 0.8
- out_recurrent: bfloat16 [1024, 2048], P('tp'), may hold values from -0.1875 to 0.1875
- out_attention: bfloat16 [1024, 2048], P('tp'), may hold values from -0.1875 to 0.1875
- out_gain: float32 [2048], replicated, may hold values from 0.1 to 1.9
Outputs:
- layer_out: bfloat16 [3072, 2048], P(('sp', 'tp'))
- log_sums: float32 [8, 2, 3072], P('tp', None, 'sp')
All inputs are finite; a program needn't handle non-finite values.
Results may differ from a plain program's by a relative error of at most 0.018.
Values may be sent and summed in bfloat16 or wider, within the bound.
A program may use at most 128 MiB of HBM per device.

v0:
```python
import functools
import math

import jax
import jax.numpy as jnp
from jax import lax
from jax.experimental import pallas as pl
from jax.experimental.pallas import tpu as pltpu
from jax.sharding import PartitionSpec as P

HD = 64
LANES = 128
CHUNK = 64
DECAY_SCALE = math.exp(-0.5)
NORM_EPS = 1e-06
GROUP_EPS = 0.00064
HEAD_EPS = 1e-05
KEY_EPS = 1e-06
NEGATIVE = -1e30
F32 = jnp.float32
BF16 = jnp.bfloat16

NN = (((1,), (0,)), ((), ()))
NT = (((1,), (1,)), ((), ()))
TN = (((0,), (0,)), ((), ()))


def dot1(a, b, dims=NN):
    return lax.dot_general(a.astype(BF16), b.astype(BF16), dims, preferred_element_type=F32)


def halves(a):
    high = a.astype(BF16)
    return high, (a - high.astype(F32)).astype(BF16)


def dot3(a, b, dims=NN):
    ah, al = halves(a)
    bh, bl = halves(b)
    one = functools.partial(lax.dot_general, dimension_numbers=dims, preferred_element_type=F32)
    return one(ah, bh) + (one(al, bh) + one(ah, bl))


def swapped(place, turn):
    bit = 1
    while bit <= turn:
        if turn & bit:
            place = place + bit - 2 * bit * lax.rem(lax.div(place, bit), 2)
        bit *= 2
    return place


def normalize(pieces, gain, normed, me):
    count = len(pieces)
    width = pieces[0].shape[1]
    wides = [piece[...].astype(F32) for piece in pieces]
    total = sum(jnp.sum(wide * wide, axis=-1, keepdims=True) for wide in wides)
    scale = lax.rsqrt(total / (width * count) + NORM_EPS)
    for turn, wide in enumerate(wides):
        columns = pl.ds(pl.multiple_of(swapped(me, turn) * width, LANES), width)
        normed[:, columns] = (wide * scale * gain[:, columns]).astype(BF16)


def recurrent_body(group, r_ref, k_ref, v_ref, d_ref, learn_ref, out_ref, turn_ref, end_ref, state):
    rows, features = r_ref.shape
    pairs = features // LANES
    lane = lax.broadcasted_iota(jnp.int32, (1, LANES), 1)
    first = (lane < HD).astype(F32)
    second = 1.0 - first
    line = lax.broadcasted_iota(jnp.int32, (LANES, LANES), 0)
    column = lax.broadcasted_iota(jnp.int32, (LANES, LANES), 1)
    strict = line > column
    causal = line >= column
    eye = (line == column).astype(F32)
    same_head = ((line // HD) == (column // HD)).astype(BF16)
    small_line = lax.broadcasted_iota(jnp.int32, (CHUNK, CHUNK), 0)
    small_column = lax.broadcasted_iota(jnp.int32, (CHUNK, CHUNK), 1)
    lower = (small_line >= small_column).astype(BF16)

    def below(size):
        return ((line // size) == (column // size) + 1) & ((line // size) % 2 == 1)

    def spread(x):
        return jnp.concatenate([x * first, x * second], axis=0)

    for pair in range(pairs):
        state[pair, :LANES, :] = jnp.zeros((LANES, LANES), F32)
        state[pair, LANES:, :] = eye

    def local(pair, at):
        here = (pl.ds(at, CHUNK), pl.ds(pair * LANES, LANES))
        r = r_ref[here].astype(F32)
        k = k_ref[here].astype(F32)
        v = v_ref[here].astype(F32)
        decay = d_ref[here]
        learn = learn_ref[:, pl.ds(pair * LANES, LANES)]
        dh = decay.astype(BF16)
        rest = decay - dh.astype(F32)
        dm = rest.astype(BF16)
        dl = (rest - dm.astype(F32)).astype(BF16)
        running = dot1(lower, dh) + (dot1(lower, dm) + dot1(lower, dl))
        before = running - decay
        middle = running[CHUNK // 2 - 1 : CHUNK // 2, :]
        ending = running[CHUNK - 1 :, :]
        sh, sl = halves(k * k)
        squares = dot1(sh, same_head) + dot1(sl, same_head)
        unit = k * lax.rsqrt(squares + KEY_EPS)
        erase = unit * learn
        rise = jnp.exp(middle - running)
        left = jnp.concatenate(
            [spread(-unit * jnp.exp(before - middle)), spread(r * jnp.exp(running - middle))], axis=0
        )
        right = jnp.concatenate([spread(erase * rise), spread(k * rise)], axis=0)
        to_end = jnp.exp(ending - running)
        return dict(
            left=left,
            right=right,
            against=spread(-unit * jnp.exp(before)),
            read=spread(r * jnp.exp(running)),
            erase_end=spread(erase * to_end),
            keys_end=spread(k * to_end),
            values=spread(v),
            whole=jnp.exp(ending),
        )

    def step(turn, carry):
        spots = [(turn * group + g, pair) for g in range(group) for pair in range(pairs)]
        items = [local(pair, pl.multiple_of(c * CHUNK, CHUNK)) for c, pair in spots]
        for it in items:
            scores = dot3(it["left"], it["right"], NT)
            it["low"] = jnp.where(strict, scores[:LANES, :LANES], 0.0)
            it["carry"] = jnp.where(strict, scores[:LANES, LANES:], 0.0)
            it["read_erase"] = jnp.where(causal, scores[LANES:, :LANES], 0.0)
            it["read_keys"] = jnp.where(causal, scores[LANES:, LANES:], 0.0)
            it["inv"] = eye + jnp.where(below(1), it["low"], 0.0)
        size = 2
        while size < CHUNK:
            keep = below(size)
            for it in items:
                it["mid"] = dot3(jnp.where(keep, it["low"], 0.0), it["inv"])
            for it in items:
                it["inv"] = it["inv"] + dot3(it["inv"], it["mid"])
            size *= 2
        for it in items:
            it["fed"] = dot3(it["carry"], it["values"])
        for it in items:
            side = jnp.concatenate([it["against"], it["fed"]], axis=1)
            it["solved"] = dot3(it["inv"], side)
        for it in items:
            seen = dot1(it["read_erase"], it["solved"])
            it["heard"] = seen[:, LANES:] + dot1(it["read_keys"], it["values"])
            it["read"] = it["read"] + seen[:, :LANES]
            it["added"] = dot3(it["values"], it["keys_end"], TN)
        for (c, pair), it in zip(spots, items):
            now = state[pair]
            both = jnp.concatenate([it["solved"][:, :LANES], it["read"]], axis=0)
            met = dot3(both, now, NT)
            gone = jnp.concatenate(
                [met[:LANES, :LANES] + it["solved"][:, LANES:], met[:LANES, LANES:]], axis=1
            )
            later = now * it["whole"] + dot3(gone, it["erase_end"], TN)
            state[pair, :LANES, :] = later[:LANES] + it["added"]
            state[pair, LANES:, :] = later[LANES:]
            heard = met[LANES:, :LANES] + it["heard"]
            turned = met[LANES:, LANES:]
            here = (pl.ds(pl.multiple_of(c * CHUNK, CHUNK), CHUNK), pl.ds(pair * LANES, LANES))
            out_ref[here] = heard[:CHUNK] + heard[CHUNK:]
            turn_ref[here] = turned[:CHUNK] + turned[CHUNK:]
        return carry

    lax.fori_loop(0, rows // CHUNK // group, step, 0)
    for pair in range(pairs):
        now = state[pair]
        end_ref[pair, :HD, :] = (now[:HD] + now[HD:LANES]).astype(BF16)
        end_ref[pair, HD:, :] = (now[LANES : LANES + HD] + now[LANES + HD :]).astype(BF16)


def finish_body(out_ref, turn_ref, ends, place, mix_ref):
    pairs = out_ref.shape[1] // LANES
    lane = lax.broadcasted_iota(jnp.int32, (1, LANES), 1)
    first = (lane < HD).astype(F32)
    second = 1.0 - first
    line = lax.broadcasted_iota(jnp.int32, (LANES, LANES), 0)
    column = lax.broadcasted_iota(jnp.int32, (LANES, LANES), 1)
    same_head = ((line // HD) == (column // HD)).astype(BF16)

    def spread(x):
        return jnp.concatenate([x * first, x * second], axis=0)

    for pair in range(pairs):
        entering = jnp.zeros((LANES, LANES), F32)
        for far, end in ends:
            block = jnp.where(place >= far, end[pair].astype(F32), 0.0)
            high, low = halves(entering)
            move = spread(block[HD:])
            entering = dot1(high, move) + dot1(low, move) + spread(block[:HD])
        columns = pl.ds(pair * LANES, LANES)
        full = out_ref[:, columns] + dot3(turn_ref[:, columns], entering, NT)

        def mean(x):
            high, low = halves(x)
            return (dot1(high, same_head) + dot1(low, same_head)) * (1.0 / HD)

        centered = full - mean(full)
        mix_ref[:, columns] = (centered * lax.rsqrt(mean(centered * centered) + GROUP_EPS)).astype(
            BF16
        )


def attend(q, blocks, valid, heads, head, at, tile, diagonal, earlier):
    lane = lax.broadcasted_iota(jnp.int32, (1, LANES), 1)
    part = q[pl.ds(at, tile), pl.ds(head * LANES, LANES)].astype(F32) * HD ** (-0.5)
    both = jnp.concatenate(
        [jnp.where(lane < HD, part, 0.0), jnp.where(lane < HD, 0.0, part)], axis=0
    ).astype(BF16)
    scores = []
    for number, (block, fine) in enumerate(zip(blocks, valid)):
        s = lax.dot_general(
            both, block[:, pl.ds(head * LANES, LANES)], NT, preferred_element_type=F32
        )
        if number == 0 and diagonal:
            line = lax.broadcasted_iota(jnp.int32, (tile, s.shape[1]), 0) + at
            seen = line >= lax.broadcasted_iota(jnp.int32, (tile, s.shape[1]), 1)
            s = jnp.where(jnp.concatenate([seen, seen], axis=0), s, NEGATIVE)
        else:
            s = jnp.where(fine, s, NEGATIVE)
        scores.append(s)
    top = functools.reduce(jnp.maximum, [jnp.max(s, axis=-1, keepdims=True) for s in scores])
    if earlier is not None:
        top = jnp.maximum(top, earlier[0])
    row_sum, acc = 0.0, 0.0
    for s, block in zip(scores, blocks):
        weights = jnp.exp(s - top)
        row_sum = row_sum + jnp.sum(weights, axis=-1, keepdims=True)
        acc = acc + jnp.dot(
            weights.astype(BF16),
            block[:, pl.ds((heads + head) * LANES, LANES)],
            preferred_element_type=F32,
        )
    if earlier is not None:
        fade = jnp.exp(earlier[0] - top)
        row_sum = row_sum + earlier[1] * fade
        acc = acc + earlier[2] * fade
    return top, row_sum, acc


def tiles_of(rows):
    tile = LANES if rows % LANES == 0 else rows
    return tile, range(0, rows, tile)


def near_body(q, blocks, place, top_ref, sum_ref, acc_ref):
    count = len(blocks)
    rows, features = q.shape
    heads = features // LANES
    tile, starts = tiles_of(rows)
    valid = [place >= 2 * turn for turn in range(count)]
    for head in range(heads):
        for at in starts:
            top, row_sum, acc = attend(q, blocks, valid, heads, head, at, tile, True, None)
            here = pl.ds(2 * at, 2 * tile)
            top_ref[head, here, :] = top
            sum_ref[head, here, :] = row_sum
            acc_ref[head, here, :] = acc


def far_body(q, lam_ref, blocks, place, top_ref, sum_ref, acc_ref, mix_ref, shift, log_ref):
    count = len(blocks)
    rows, features = q.shape
    heads = features // LANES
    other = swapped(place, 1)
    tile, starts = tiles_of(rows)
    valid = [(other >= 2 * turn) & (other - 2 * turn < place) for turn in range(count)]
    for head in range(heads):
        lam = lam_ref[head]
        for at in starts:
            here = pl.ds(2 * at, 2 * tile)
            earlier = (top_ref[head, here, :], sum_ref[head, here, :], acc_ref[head, here, :])
            top, row_sum, acc = attend(q, blocks, valid, heads, head, at, tile, False, earlier)
            maps = acc / row_sum
            logs = top + jnp.log(row_sum)
            flat = jnp.transpose(jnp.broadcast_to(logs, (2 * tile, LANES)))
            log_ref[head, 0:1, pl.ds(at, tile)] = flat[:1, :tile]
            log_ref[head, 1:2, pl.ds(at, tile)] = flat[:1, tile:]
            out = maps[:tile] - lam * maps[tile:]
            out = out * lax.rsqrt(jnp.mean(out * out, axis=-1, keepdims=True) + HEAD_EPS)
            mix_ref[pl.ds(at, tile), pl.ds(shift + head * LANES, LANES)] = out.astype(BF16)


def layer_body(sp, tp, *refs):
    (hidden, gain, wr_h, wk_h, wv_h, down_h, up_h, base, shift, learn) = refs[:10]
    (wq_h, wkp_h, wvp_h, lam, rec_h, att_h, out_gain, out, logs) = refs[10:19]
    (xs, normed, wr, wk, wv, down, up, wq, wkp, wvp, hw) = refs[19:30]
    (near, far, r, k, v, d, q, heard, turned, ends, state) = refs[30:41]
    (top, row_sum, acc, mix, moved) = refs[41:46]
    (load, x_send, x_recv, w_send, w_recv, n_send, n_recv) = refs[46:53]
    (f_send, f_recv, e_send, e_recv, m_send, m_recv) = refs[53:]
    rows, features = r.shape
    wide = q.shape[1]
    me = lax.axis_index("tp")
    place = lax.axis_index("sp")
    count = sp // 2

    barrier = pltpu.get_barrier_semaphore()
    for turn in range(1, tp):
        pl.semaphore_signal(barrier, inc=1, device_id={"tp": swapped(me, turn)})
    for hop in range(1, sp):
        pl.semaphore_signal(barrier, inc=1, device_id={"sp": lax.rem(place + hop, sp)})
    loads = []
    for number, (source, target) in enumerate(
        (
            (wkp_h, wkp),
            (wvp_h, wvp),
            (wq_h, wq),
            (wr_h, wr),
            (wk_h, wk),
            (wv_h, wv),
            (down_h, down),
            (up_h, up),
            (rec_h, hw.at[0, pl.ds(0, features)]),
            (att_h, hw.at[0, pl.ds(features, wide)]),
        )
    ):
        loads.append(pltpu.make_async_copy(source, target, load.at[number]))
        loads[-1].start()
    pl.semaphore_wait(barrier, tp - 1 + sp - 1)

    def remote(source, target, send, recv, slot, device):
        return pltpu.make_async_remote_copy(
            src_ref=source,
            dst_ref=target,
            send_sem=send.at[slot],
            recv_sem=recv.at[slot],
            device_id=device,
        )

    def spreading(own, slots, send, recv):
        def source(turn):
            return own if turn == 0 else slots.at[turn]

        copies = {}
        for turn in range(1, tp):
            if turn % 2 == 0:
                copies[turn] = remote(
                    own, slots.at[turn], send, recv, turn, {"tp": swapped(me, turn)}
                )
            else:
                copies[turn] = remote(
                    source(turn - 1), slots.at[turn], send, recv, turn, {"tp": swapped(me, 1)}
                )
        return copies

    hops = spreading(hidden, xs, x_send, x_recv)
    for turn in range(2, tp, 2):
        hops[turn].start()
    hops[1].start()
    for turn in range(2, tp, 2):
        hops[turn].wait_recv()
        hops[turn + 1].start()
    for turn in range(1, tp, 2):
        hops[turn].wait_recv()
    loads[8].wait()
    loads[9].wait()
    outs = spreading(hw.at[0], hw, w_send, w_recv)
    for turn in range(2, tp, 2):
        outs[turn].start()
    outs[1].start()
    normalize([hidden] + [xs.at[turn] for turn in range(1, tp)], gain, normed, me)

    def product(weight):
        return jnp.dot(normed[...], weight[...], preferred_element_type=F32)

    for one in loads[:8]:
        one.wait()
    near[0, :, :wide] = product(wkp).astype(BF16)
    near[0, :, wide:] = product(wvp).astype(BF16)
    q[...] = product(wq).astype(BF16)
    nears = {
        turn: remote(
            near.at[0],
            near.at[turn],
            n_send,
            n_recv,
            turn,
            {"sp": lax.rem(place + 2 * turn, sp)},
        )
        for turn in range(1, count)
    }
    fars = [
        remote(near.at[turn], far.at[turn], f_send, f_recv, turn, {"sp": swapped(place, 1)})
        for turn in range(count)
    ]
    for turn in range(1, count):
        nears[turn].start()
    fars[0].start()
    r[...] = product(wr).astype(BF16)
    k[...] = product(wk).astype(BF16)
    v[...] = product(wv).astype(BF16)
    low_rank = jnp.tanh(product(down)).astype(BF16)
    pre = jnp.dot(low_rank, up[...], preferred_element_type=F32) + base[...]
    d[...] = -DECAY_SCALE * jax.nn.sigmoid(pre) + shift[...]

    group = 2 if (rows // CHUNK) % 2 == 0 else 1
    recurrent_body(group, r, k, v, d, learn, heard, turned, ends.at[0], state)
    states = {
        hop: remote(
            ends.at[0], ends.at[hop], e_send, e_recv, hop, {"sp": lax.rem(place + hop, sp)}
        )
        for hop in range(1, sp)
    }
    for hop in range(1, sp):
        states[hop].start()
    for turn in range(1, count):
        nears[turn].wait_recv()
        fars[turn].start()
    near_body(q, [near.at[turn] for turn in range(count)], place, top, row_sum, acc)
    for hop in range(1, sp):
        states[hop].wait_recv()
    finish_body(
        heard, turned, [(hop, ends.at[hop]) for hop in range(sp - 1, 0, -1)], place, mix
    )
    for turn in range(2, tp, 2):
        outs[turn].wait_recv()
        outs[turn + 1].start()
    for turn in range(count):
        fars[turn].wait_recv()
    far_body(
        q,
        lam,
        [far.at[turn] for turn in range(count)],
        place,
        top,
        row_sum,
        acc,
        mix,
        features,
        logs,
    )
    part = rows // tp
    mixes = {}
    for turn in range(1, tp):
        owner = swapped(me, turn)
        mixes[turn] = remote(
            mix.at[pl.ds(pl.multiple_of(owner * part, part), part)],
            moved.at[turn],
            m_send,
            m_recv,
            turn,
            {"tp": owner},
        )
    for turn in list(range(2, tp)) + [1]:
        mixes[turn].start()
    total = jnp.dot(
        mix[pl.ds(pl.multiple_of(me * part, part), part), :], hw[0], preferred_element_type=F32
    )
    for turn in range(1, tp):
        mixes[turn].wait_recv()
        if turn % 2:
            outs[turn].wait_recv()
        total = total + jnp.dot(moved[turn], hw[turn], preferred_element_type=F32)
    mean = jnp.mean(total * total, axis=-1, keepdims=True)
    out[...] = (total * lax.rsqrt(mean + NORM_EPS) * out_gain[...]).astype(BF16)
    for group_of in (hops, outs, nears, states, mixes):
        for one in group_of.values():
            one.wait_send()
    for one in fars:
        one.wait_send()


def per_device(
    sp,
    tp,
    hidden_in,
    in_gain,
    receptance_weight,
    key_weight,
    value_weight,
    decay_down,
    decay_up,
    decay_base,
    decay_shift,
    learn_rate,
    query_pair,
    key_pair,
    value_pair,
    mix_lambda,
    out_recurrent,
    out_attention,
    out_gain,
):
    rows, width = hidden_in.shape
    depth = width * tp
    features = receptance_weight.shape[1]
    heads = mix_lambda.shape[0]
    wide = heads * LANES
    pairs = features // LANES
    low = decay_down.shape[1]
    across = out_recurrent.shape[1]
    part = rows // tp
    count = sp // 2
    shape = jax.ShapeDtypeStruct
    held = pltpu.VMEM
    args = (
        hidden_in,
        in_gain.reshape(1, -1),
        receptance_weight,
        key_weight,
        value_weight,
        decay_down,
        decay_up,
        decay_base.reshape(1, -1),
        decay_shift,
        learn_rate.reshape(1, -1),
        query_pair.reshape(depth, wide),
        key_pair.reshape(depth, wide),
        value_pair.reshape(depth, wide),
        mix_lambda,
        out_recurrent,
        out_attention,
        out_gain.reshape(1, -1),
    )
    inside = pl.BlockSpec(memory_space=pltpu.VMEM)
    outside = pl.BlockSpec(memory_space=pl.ANY)
    specs = [inside] * 2 + [outside] * 5 + [inside] * 3 + [outside] * 3
    specs += [pl.BlockSpec(memory_space=pltpu.SMEM)] + [outside] * 2 + [inside]
    sizes = (10, tp, tp, tp, tp, count, count, count, count, sp, sp, tp, tp)
    return tuple(
        pl.pallas_call(
            functools.partial(layer_body, sp, tp),
            out_shape=[shape((part, across), BF16), shape((heads, 2, rows), F32)],
            in_specs=specs,
            out_specs=[inside] * 2,
            scratch_shapes=[
                held((tp, rows, width), BF16),
                held((rows, depth), BF16),
                held((depth, features), BF16),
                held((depth, features), BF16),
                held((depth, features), BF16),
                held((depth, low), BF16),
                held((low, features), BF16),
                held((depth, wide), BF16),
                held((depth, wide), BF16),
                held((depth, wide), BF16),
                held((tp, features + wide, across), BF16),
                held((count, rows, 2 * wide), BF16),
                held((count, rows, 2 * wide), BF16),
                held((rows, features), BF16),
                held((rows, features), BF16),
                held((rows, features), BF16),
                held((rows, features), F32),
                held((rows, wide), BF16),
                held((rows, features), F32),
                held((rows, features), F32),
                held((sp, pairs, 2 * HD, LANES), BF16),
                held((pairs, 2 * LANES, LANES), F32),
                held((heads, 2 * rows, 1), F32),
                held((heads, 2 * rows, 1), F32),
                held((heads, 2 * rows, LANES), F32),
                held((rows, features + wide), BF16),
                held((tp, part, features + wide), BF16),
            ]
            + [pltpu.SemaphoreType.DMA((size,)) for size in sizes],
            compiler_params=pltpu.CompilerParams(
                collective_id=0, has_side_effects=True, vmem_limit_bytes=62 * 1024 * 1024
            ),
        )(*args)
    )


def solution(mesh):
    in_specs = (
        P("sp", "tp"),
        P(),
        P(None, "tp"),
        P(None, "tp"),
        P(None, "tp"),
        P(),
        P(None, "tp"),
        P("tp"),
        P("sp", "tp"),
        P("tp"),
        P(None, "tp", None),
        P(None, "tp", None),
        P(None, "tp", None),
        P("tp"),
        P("tp", None),
        P("tp", None),
        P(),
    )
    out_specs = (P(("sp", "tp"), None), P("tp", None, "sp"))
    body = functools.partial(per_device, mesh.shape["sp"], mesh.shape["tp"])
    return jax.shard_map(
        body, mesh=mesh, in_specs=in_specs, out_specs=out_specs, check_vma=False
    )
```

profile of v0, /device:TPU:25, one launch (start us, length us, event | category | flops | bytes accessed | tf_op | source)
XLA Modules:
  0.0 97.8 jit_solution(13498317929345151424)
XLA Ops:
  0.6 0.0 copy-start
  0.6 0.0 copy-start.1
  0.7 2.5 %copy.25 = bf16[256,8,2,128]{3,1,2,0:T(8,128)(2,1)} copy(bf16[256,8,2,128]{3,2,1,0:T(2,128)(2,1)} %bitcast.15) | data formatting | bytes 2097152
  3.1 0.0 copy-done
  3.1 0.0 copy-done.1
  3.1 1.7 %copy_bitcast_fusion = (bf16[2048,256]{1,0:T(8,128)(2,1)}, bf16[2048,256]{1,0:T(8,128)(2,1)}) fusion(bf16[256,8,2,128]{3,2,1,0:T(2,128)(2,1)S(1)} %bitcast.16, bf16[256,8,2,128]{3,2,1,0:T(2,128)(2,1)S(1)} %bitcast.17), kind=kLoop, calls=%fused_computation | loop fusion | bytes 4194304 | tf_op jit(solution)/shard_map/reshape | solution.py:516
  4.9 90.5 %shard_map.176 = (bf16[96,2048]{1,0:T(8,128)(2,1)}, f32[2,2,384]{2,1,0:T(2,128)}) custom-call(bf16[384,512]{1,0:T(8,128)(2,1)} %refs_0_.1, f32[1,2048]{1,0:T(1,128)} %bitcast.18, bf16[2048,256]{1,0:T(8,128)(2,1)} %refs_2_.1, bf16[2048,256]{1,0:T(8,128)(2,1)} %refs_3_.1, bf16[2048,256]{1,0:T(8,128)(2,1)} %refs_4_.1, bf16[2048,128]{1,0:T(8,128)(2,1)} %refs_5_.1, ...), custom_call_target="tpu_custom_call" | custom-call | tf_op jit(solution)/shard_map/pallas_call | solution.py:528
  95.4 0.0 copy-start.2
  95.4 1.8 %copy.28 = bf16[96,2048]{1,0:T(8,128)(2,1)} copy(bf16[96,2048]{1,0:T(8,128)(2,1)} %get-tuple-element.6) | data formatting | bytes 786432
  97.2 0.0 copy-done.2
  97.2 0.6 copy.29
Async XLA Ops:
  0.6 2.5 %copy-start = (bf16[2048,2,128]{2,1,0:T(2,128)(2,1)S(1)}, bf16[2048,2,128]{2,1,0:T(2,128)(2,1)}, u32[]{:S(2)}) copy-start(bf16[2048,2,128]{2,1,0:T(2,128)(2,1)} %param.29) | copy-start | bytes 3145732
  0.6 2.5 %copy-start.1 = (bf16[2048,2,128]{2,1,0:T(2,128)(2,1)S(1)}, bf16[2048,2,128]{2,1,0:T(2,128)(2,1)}, u32[]{:S(2)}) copy-start(bf16[2048,2,128]{2,1,0:T(2,128)(2,1)} %param.28) | copy-start | bytes 3145732
  95.4 1.8 %copy-start.2 = (f32[2,2,384]{2,1,0:T(2,128)S(1)}, f32[2,2,384]{2,1,0:T(2,128)}, u32[]{:S(2)}) copy-start(f32[2,2,384]{2,1,0:T(2,128)} %get-tuple-element.7) | copy-start | bytes 18436
where the time goes:
time: 97.9 us; the launch traced here: 97.8 us
  Pallas kernels  90.5 us (92%)
  local copies, waits for them, and re-layouts  6.6 us (7%)
    pallas_call x1, Pallas kernels, per_device(): pl.pallas_call(functools.partial(layer_body, sp, tp), out_shape=[shape((p...  90.5 us
    unnamed x9, local copies, waits for them, and re-layouts  4.85 us

commit v1 on v0

v1 whole, which is shorter than its diff:
```python
import functools
import math

import jax
import jax.numpy as jnp
from jax import lax
from jax.experimental import pallas as pl
from jax.experimental.pallas import tpu as pltpu
from jax.sharding import PartitionSpec as P

HD = 64
LANES = 128
CHUNK = 64
DECAY_SCALE = math.exp(-0.5)
NORM_EPS = 1e-06
GROUP_EPS = 0.00064
HEAD_EPS = 1e-05
KEY_EPS = 1e-06
NEGATIVE = -1e30
F32 = jnp.float32
BF16 = jnp.bfloat16

NN = (((1,), (0,)), ((), ()))
NT = (((1,), (1,)), ((), ()))
TN = (((0,), (0,)), ((), ()))


def dot1(a, b, dims=NN):
    return lax.dot_general(a.astype(BF16), b.astype(BF16), dims, preferred_element_type=F32)


def halves(a):
    high = a.astype(BF16)
    return high, (a - high.astype(F32)).astype(BF16)


def dot3(a, b, dims=NN):
    ah, al = halves(a)
    bh, bl = halves(b)
    one = functools.partial(lax.dot_general, dimension_numbers=dims, preferred_element_type=F32)
    return one(ah, bh) + (one(al, bh) + one(ah, bl))


def swapped(place, turn):
    bit = 1
    while bit <= turn:
        if turn & bit:
            place = place + bit - 2 * bit * lax.rem(lax.div(place, bit), 2)
        bit *= 2
    return place


def normalize(pieces, gain, normed, me, here):
    count = len(pieces)
    width = pieces[0].shape[1]
    wides = [piece[here, :].astype(F32) for piece in pieces]
    total = sum(jnp.sum(wide * wide, axis=-1, keepdims=True) for wide in wides)
    scale = lax.rsqrt(total / (width * count) + NORM_EPS)
    for turn, wide in enumerate(wides):
        columns = pl.ds(pl.multiple_of(swapped(me, turn) * width, LANES), width)
        normed[here, columns] = (wide * scale * gain[:, columns]).astype(BF16)


def recurrent_body(group, between, r_ref, k_ref, v_ref, d_ref, learn_ref, out_ref, turn_ref, end_ref, state):
    rows, features = r_ref.shape
    pairs = features // LANES
    lane = lax.broadcasted_iota(jnp.int32, (1, LANES), 1)
    first = (lane < HD).astype(F32)
    second = 1.0 - first
    line = lax.broadcasted_iota(jnp.int32, (LANES, LANES), 0)
    column = lax.broadcasted_iota(jnp.int32, (LANES, LANES), 1)
    strict = line > column
    causal = line >= column
    eye = (line == column).astype(F32)
    same_head = ((line // HD) == (column // HD)).astype(BF16)
    small_line = lax.broadcasted_iota(jnp.int32, (CHUNK, CHUNK), 0)
    small_column = lax.broadcasted_iota(jnp.int32, (CHUNK, CHUNK), 1)
    lower = (small_line >= small_column).astype(BF16)

    def below(size):
        return ((line // size) == (column // size) + 1) & ((line // size) % 2 == 1)

    def spread(x):
        return jnp.concatenate([x * first, x * second], axis=0)

    for pair in range(pairs):
        state[pair, :LANES, :] = jnp.zeros((LANES, LANES), F32)
        state[pair, LANES:, :] = eye

    def local(pair, at):
        here = (pl.ds(at, CHUNK), pl.ds(pair * LANES, LANES))
        r = r_ref[here].astype(F32)
        k = k_ref[here].astype(F32)
        v = v_ref[here].astype(F32)
        decay = d_ref[here]
        learn = learn_ref[:, pl.ds(pair * LANES, LANES)]
        dh = decay.astype(BF16)
        rest = decay - dh.astype(F32)
        dm = rest.astype(BF16)
        dl = (rest - dm.astype(F32)).astype(BF16)
        running = dot1(lower, dh) + (dot1(lower, dm) + dot1(lower, dl))
        before = running - decay
        middle = running[CHUNK // 2 - 1 : CHUNK // 2, :]
        ending = running[CHUNK - 1 :, :]
        sh, sl = halves(k * k)
        squares = dot1(sh, same_head) + dot1(sl, same_head)
        unit = k * lax.rsqrt(squares + KEY_EPS)
        erase = unit * learn
        rise = jnp.exp(middle - running)
        left = jnp.concatenate(
            [spread(-unit * jnp.exp(before - middle)), spread(r * jnp.exp(running - middle))], axis=0
        )
        right = jnp.concatenate([spread(erase * rise), spread(k * rise)], axis=0)
        to_end = jnp.exp(ending - running)
        return dict(
            left=left,
            right=right,
            against=spread(-unit * jnp.exp(before)),
            read=spread(r * jnp.exp(running)),
            erase_end=spread(erase * to_end),
            keys_end=spread(k * to_end),
            values=spread(v),
            whole=jnp.exp(ending),
        )

    def step(turn, carry):
        between(turn)
        spots = [(turn * group + g, pair) for g in range(group) for pair in range(pairs)]
        items = [local(pair, pl.multiple_of(c * CHUNK, CHUNK)) for c, pair in spots]
        for it in items:
            scores = dot3(it["left"], it["right"], NT)
            it["low"] = jnp.where(strict, scores[:LANES, :LANES], 0.0)
            it["carry"] = jnp.where(strict, scores[:LANES, LANES:], 0.0)
            it["read_erase"] = jnp.where(causal, scores[LANES:, :LANES], 0.0)
            it["read_keys"] = jnp.where(causal, scores[LANES:, LANES:], 0.0)
            it["inv"] = eye + jnp.where(below(1), it["low"], 0.0)
        size = 2
        while size < CHUNK:
            keep = below(size)
            for it in items:
                it["mid"] = dot3(jnp.where(keep, it["low"], 0.0), it["inv"])
            for it in items:
                it["inv"] = it["inv"] + dot3(it["inv"], it["mid"])
            size *= 2
        for it in items:
            it["fed"] = dot3(it["carry"], it["values"])
        for it in items:
            side = jnp.concatenate([it["against"], it["fed"]], axis=1)
            it["solved"] = dot3(it["inv"], side)
        for it in items:
            seen = dot1(it["read_erase"], it["solved"])
            it["heard"] = seen[:, LANES:] + dot1(it["read_keys"], it["values"])
            it["read"] = it["read"] + seen[:, :LANES]
            it["added"] = dot3(it["values"], it["keys_end"], TN)
        for (c, pair), it in zip(spots, items):
            now = state[pair]
            both = jnp.concatenate([it["solved"][:, :LANES], it["read"]], axis=0)
            met = dot3(both, now, NT)
            gone = jnp.concatenate(
                [met[:LANES, :LANES] + it["solved"][:, LANES:], met[:LANES, LANES:]], axis=1
            )
            later = now * it["whole"] + dot3(gone, it["erase_end"], TN)
            state[pair, :LANES, :] = later[:LANES] + it["added"]
            state[pair, LANES:, :] = later[LANES:]
            heard = met[LANES:, :LANES] + it["heard"]
            turned = met[LANES:, LANES:]
            here = (pl.ds(pl.multiple_of(c * CHUNK, CHUNK), CHUNK), pl.ds(pair * LANES, LANES))
            out_ref[here] = heard[:CHUNK] + heard[CHUNK:]
            turn_ref[here] = turned[:CHUNK] + turned[CHUNK:]
        return carry

    lax.fori_loop(0, rows // CHUNK // group, step, 0)
    for pair in range(pairs):
        now = state[pair]
        end_ref[pair, :HD, :] = (now[:HD] + now[HD:LANES]).astype(BF16)
        end_ref[pair, HD:, :] = (now[LANES : LANES + HD] + now[LANES + HD :]).astype(BF16)


def finish_body(out_ref, turn_ref, ends, place, mix_ref):
    pairs = out_ref.shape[1] // LANES
    lane = lax.broadcasted_iota(jnp.int32, (1, LANES), 1)
    first = (lane < HD).astype(F32)
    second = 1.0 - first
    line = lax.broadcasted_iota(jnp.int32, (LANES, LANES), 0)
    column = lax.broadcasted_iota(jnp.int32, (LANES, LANES), 1)
    same_head = ((line // HD) == (column // HD)).astype(BF16)

    def spread(x):
        return jnp.concatenate([x * first, x * second], axis=0)

    for pair in range(pairs):
        entering = jnp.zeros((LANES, LANES), F32)
        for far, end in ends:
            block = jnp.where(place >= far, end[pair].astype(F32), 0.0)
            high, low = halves(entering)
            move = spread(block[HD:])
            entering = dot1(high, move) + dot1(low, move) + spread(block[:HD])
        columns = pl.ds(pair * LANES, LANES)
        full = out_ref[:, columns] + dot3(turn_ref[:, columns], entering, NT)

        def mean(x):
            high, low = halves(x)
            return (dot1(high, same_head) + dot1(low, same_head)) * (1.0 / HD)

        centered = full - mean(full)
        mix_ref[pair] = (centered * lax.rsqrt(mean(centered * centered) + GROUP_EPS)).astype(
            BF16
        )


def update(queries, at, tile, blocks, mask, tops, sums, accs):
    here = pl.ds(2 * at, 2 * tile)
    lhs = queries[here, :]
    scores = [
        lax.dot_general(lhs, keys, NT, preferred_element_type=F32) for keys, _ in blocks
    ]
    if mask is not None:
        scores = [jnp.where(mask, s, NEGATIVE) for s in scores]
    old = tops[here, :]
    top = functools.reduce(jnp.maximum, [jnp.max(s, axis=-1, keepdims=True) for s in scores])
    top = jnp.maximum(top, old)
    fade = jnp.exp(old - top)
    row_sum = sums[here, :] * fade
    acc = accs[here, :] * fade
    for s, (_, values) in zip(scores, blocks):
        weights = jnp.exp(s - top)
        row_sum = row_sum + jnp.sum(weights, axis=-1, keepdims=True)
        acc = acc + jnp.dot(weights.astype(BF16), values, preferred_element_type=F32)
    return here, top, row_sum, acc


def attend(q, kv, head, index, lam, queries, tops, sums, accs, mix_ref, log_ref):
    rows = q.shape[0]
    tile = LANES if rows % LANES == 0 else rows
    starts = range(0, rows, tile)
    lane = lax.broadcasted_iota(jnp.int32, (1, LANES), 1)
    for at in starts:
        part = q[pl.ds(at, tile), :].astype(F32) * HD ** (-0.5)
        queries[pl.ds(2 * at, 2 * tile), :] = jnp.concatenate(
            [jnp.where(lane < HD, part, 0.0), jnp.where(lane < HD, 0.0, part)], axis=0
        ).astype(BF16)
    tops[...] = jnp.full(tops.shape, NEGATIVE, F32)
    sums[...] = jnp.zeros(sums.shape, F32)
    accs[...] = jnp.zeros(accs.shape, F32)

    def fold(numbers):
        blocks = [(kv[n, head, :, :LANES], kv[n, head, :, LANES:]) for n in numbers]
        for at in starts:
            here, top, row_sum, acc = update(
                queries, at, tile, blocks, None, tops, sums, accs
            )
            tops[here, :] = top
            sums[here, :] = row_sum
            accs[here, :] = acc

    def both(turn, carry):
        fold([2 * turn, 2 * turn + 1])
        return carry

    lax.fori_loop(0, lax.div(index, 2), both, 0)
    pl.when(lax.rem(index, 2) == 1)(lambda: fold([index - 1]))
    for at in starts:
        size = at + tile
        line = lax.broadcasted_iota(jnp.int32, (tile, size), 0) + at
        seen = line >= lax.broadcasted_iota(jnp.int32, (tile, size), 1)
        block = (kv[index, head, :size, :LANES], kv[index, head, :size, LANES:])
        mask = jnp.concatenate([seen, seen], axis=0)
        _, top, row_sum, acc = update(queries, at, tile, [block], mask, tops, sums, accs)
        maps = acc / row_sum
        logs = top + jnp.log(row_sum)
        flat = jnp.transpose(jnp.broadcast_to(logs, (2 * tile, LANES)))
        log_ref[0:1, pl.ds(at, tile)] = flat[:1, :tile]
        log_ref[1:2, pl.ds(at, tile)] = flat[:1, tile:]
        out = maps[:tile] - lam * maps[tile:]
        out = out * lax.rsqrt(jnp.mean(out * out, axis=-1, keepdims=True) + HEAD_EPS)
        mix_ref[pl.ds(at, tile), :] = out.astype(BF16)


def layer_body(sp, tp, *refs):
    (hidden, gain, wr_h, wk_h, wv_h, down_h, up_h, base, shift, learn) = refs[:10]
    (wq_h, wkp_h, wvp_h, lam, rec_h, att_h, out_gain, out, logs) = refs[10:19]
    (xs, normed, wr, wk, wv, down, up, wq, wkp, wvp, hw) = refs[19:30]
    (wq_p, wkp_p, wvp_p, kv, r, k, v, d, q, heard, turned, ends, state) = refs[30:43]
    (queries, top, row_sum, acc, mix, moved, q_far, mix_far, log_far) = refs[43:52]
    (log_got, total, parts, got) = refs[52:56]
    (load, x_send, x_recv, w_send, w_recv, z_send, z_recv, c_send, c_recv) = refs[56:65]
    (e_send, e_recv, q_send, q_recv, b_send, b_recv, m_send, m_recv) = refs[65:73]
    (p_send, p_recv) = refs[73:]
    rows, features = r.shape
    heads = q.shape[0]
    wide = heads * LANES
    pairs = features // LANES
    me = lax.axis_index("tp")
    place = lax.axis_index("sp")
    count = sp // 2
    level = lax.div(place, 2)
    across = swapped(place, 1)
    mirror = sp - 1 - place
    early = place < count
    late = place >= count
    moving = list(range(heads - heads // 2, heads))
    staying = list(range(heads - heads // 2))
    parts_of = z_recv.shape[2]
    piece = rows // parts_of

    barrier = pltpu.get_barrier_semaphore()
    for turn in range(1, tp):
        pl.semaphore_signal(barrier, inc=1, device_id={"tp": swapped(me, turn)})
    for hop in range(1, sp):
        pl.semaphore_signal(barrier, inc=1, device_id={"sp": lax.rem(place + hop, sp)})
    pair_loads = heads > 1
    loads = []
    for number, (source, target) in enumerate(
        (
            (wkp_h, wkp_p if pair_loads else wkp),
            (wvp_h, wvp_p if pair_loads else wvp),
            (wq_h, wq_p if pair_loads else wq),
            (wr_h, wr),
            (wk_h, wk),
            (wv_h, wv),
            (down_h, down),
            (up_h, up),
            (rec_h, hw.at[0, pl.ds(0, features)]),
            (att_h, hw.at[0, pl.ds(features, wide)]),
        )
    ):
        loads.append(pltpu.make_async_copy(source, target, load.at[number]))
        loads[-1].start()
    pl.semaphore_wait(barrier, tp - 1 + sp - 1)

    def remote(source, target, send, recv, device):
        return pltpu.make_async_remote_copy(
            src_ref=source, dst_ref=target, send_sem=send, recv_sem=recv, device_id=device
        )

    chunks = [pl.ds(number * piece, piece) for number in range(parts_of)]
    hops = {}
    for turn in range(1, tp):
        for number, here in enumerate(chunks):
            source = hidden if turn < 2 or turn % 2 == 0 else xs.at[turn - 1]
            hops[turn, number] = remote(
                source.at[here],
                xs.at[turn, here],
                x_send.at[turn, number],
                x_recv.at[turn, number],
                {"tp": swapped(me, turn if turn % 2 == 0 else 1)},
            )
    for number in range(parts_of):
        for turn in range(2, tp, 2):
            hops[turn, number].start()
        hops[1, number].start()

    def unpack(packed, target):
        def one(turn, carry):
            lines = pl.ds(pl.multiple_of(turn * 256, 256), 256)
            for head in range(heads):
                target[lines, pl.ds(head * LANES, LANES)] = packed[lines, head, :]
            return carry

        lax.fori_loop(0, target.shape[0] // 256, one, 0)

    for one in loads[:3]:
        one.wait()
    if pair_loads:
        unpack(wkp_p, wkp)
        unpack(wvp_p, wvp)
        unpack(wq_p, wq)

    def column(head, source, target, number):
        here = kv.at[source, head, chunks[number]]
        return remote(
            here,
            here,
            z_send.at[head, target, number],
            z_recv.at[head, source_level(source), number],
            {"sp": 2 * target + lax.rem(place, 2)},
        )

    def source_level(source):
        return lax.div(source, 2)

    def crossing(head, source, number):
        here = kv.at[source, head, chunks[number]]
        return remote(
            here,
            here,
            c_send.at[head, source_level(source), number],
            c_recv.at[head, source_level(source), number],
            {"sp": across},
        )

    def column_goes():
        plan = []
        for target in range(count - 1, -1, -1):
            for head in staying:
                plan.append((head, target, target > level))
            if target < count // 2:
                for head in moving:
                    plan.append((head, target, (target != level) & (level <= count - 1 - target)))
        return plan

    own_crosses = [(head, lax.rem(place, 2) == 0) for head in staying] + [
        (head, level < count // 2) for head in moving
    ]
    relayed = []
    for far in range(1, count):
        stage = []
        for head in staying:
            stage.append((head, level - far, level >= far))
        for head in moving:
            stage.append(
                (head, level + far, (level < count // 2) & (level + far <= count - 1 - level))
            )
            stage.append((head, level - far, (level < count // 2) & (level >= far)))
        relayed.append(stage)

    def guarded(condition, work):
        pl.when(condition)(work)

    def send_piece(number):
        for head, condition in own_crosses:
            guarded(condition, lambda head=head: crossing(head, place, number).start())
        for head, target, condition in column_goes():
            guarded(
                condition,
                lambda head=head, target=target: column(head, place, target, number).start(),
            )

    def relay(stage):
        for head, source, condition in relayed[stage]:

            def one(head=head, source=source):
                slot = 2 * source + lax.rem(place, 2)
                for number in range(parts_of):
                    column(head, slot, level, number).wait_recv()
                    crossing(head, slot, number).start()

            guarded(condition, one)

    def product(here, weight):
        return jnp.dot(normed[here, :], weight[...], preferred_element_type=F32)

    for number, here in enumerate(chunks):
        for turn in range(2, tp, 2):
            hops[turn, number].wait_recv()
            hops[turn + 1, number].start()
        for turn in range(1, tp, 2):
            hops[turn, number].wait_recv()
        normalize([hidden] + [xs.at[turn] for turn in range(1, tp)], gain, normed, me, here)
        keys = product(here, wkp).astype(BF16)
        values = product(here, wvp).astype(BF16)
        for head in range(heads):
            columns = slice(head * LANES, (head + 1) * LANES)
            kv[place, head, here, :LANES] = keys[:, columns]
            kv[place, head, here, LANES:] = values[:, columns]
        send_piece(number)
        if number == 0:
            for one in loads[3:]:
                one.wait()
            outs = remote(
                hw.at[0], hw.at[1], w_send.at[0], w_recv.at[0], {"tp": swapped(me, 1)}
            )
            outs.start()
        mine = product(here, wq).astype(BF16)
        for head in range(heads):
            q[head, here, :] = mine[:, head * LANES : (head + 1) * LANES]
        r[here, :] = product(here, wr).astype(BF16)
        k[here, :] = product(here, wk).astype(BF16)
        v[here, :] = product(here, wv).astype(BF16)
        low_rank = jnp.tanh(product(here, down)).astype(BF16)
        pre = jnp.dot(low_rank, up[...], preferred_element_type=F32) + base[...]
        d[here, :] = -DECAY_SCALE * jax.nn.sigmoid(pre) + shift[here, :]

    asks = [
        remote(q.at[head], q_far.at[n], q_send.at[n], q_recv.at[n], {"sp": mirror})
        for n, head in enumerate(moving)
    ]
    if moving:
        guarded(late, lambda: [one.start() for one in asks] and None)

    group = 2 if (rows // CHUNK) % 2 == 0 else 1
    turns = rows // CHUNK // group
    placed = {}
    for stage in range(count - 1):
        placed.setdefault(min(stage + 1, turns), []).append(stage)

    def between(turn):
        for when, stages in placed.items():
            if when < turns:

                def work(stages=stages):
                    for stage in stages:
                        relay(stage)

                pl.when(turn == when)(work)

    recurrent_body(group, between, r, k, v, d, learn, heard, turned, ends.at[0], state)
    states = {
        hop: remote(
            ends.at[0], ends.at[hop], e_send.at[hop], e_recv.at[hop], {"sp": place + hop}
        )
        for hop in range(1, sp)
    }
    for hop in range(1, sp):
        guarded(place + hop < sp, states[hop].start)
    for stage in placed.get(turns, []):
        relay(stage)

    def arrive(names, last):
        for source in range(count):
            for side in range(2):
                slot = 2 * source + side

                def one(slot=slot):
                    for head in names:
                        for number in range(parts_of):
                            crossing(head, slot, number).wait_recv()

                guarded((lax.rem(place, 2) != side) & (slot <= last), one)

    answers = []
    for n, head in enumerate(moving):
        answers.append(
            remote(
                mix_far.at[n],
                mix.at[pairs + head],
                b_send.at[n, 0],
                b_recv.at[n, 0],
                {"sp": mirror},
            )
        )
        answers.append(
            remote(
                log_far.at[n], log_got.at[n], b_send.at[n, 1], b_recv.at[n, 1], {"sp": mirror}
            )
        )
    work = (queries, top, row_sum, acc)

    if moving:

        def foreign():
            arrive(moving, mirror)
            for n, head in enumerate(moving):
                asks[n].wait_recv()
                attend(
                    q_far.at[n], kv, head, mirror, lam[head], *work, mix_far.at[n], log_far.at[n]
                )
                answers[2 * n].start()
                answers[2 * n + 1].start()

        guarded(early, foreign)
    arrive(staying, place)
    for head in staying:
        attend(
            q.at[head], kv, head, place, lam[head], *work, mix.at[pairs + head], logs.at[head]
        )
    if moving:

        def local():
            for head in moving:
                attend(
                    q.at[head],
                    kv,
                    head,
                    place,
                    lam[head],
                    *work,
                    mix.at[pairs + head],
                    logs.at[head],
                )

        guarded(early, local)
    for hop in range(1, sp):
        guarded(place >= hop, states[hop].wait_recv)
    finish_body(
        heard, turned, [(hop, ends.at[hop]) for hop in range(sp - 1, 0, -1)], place, mix
    )
    if moving:

        def collect():
            for one in answers:
                one.wait_recv()
            for n, head in enumerate(moving):
                logs[head] = log_got[n]

        guarded(late, collect)

    part = rows // tp
    mate = swapped(me, 1)

    def lines(owner):
        return pl.ds(pl.multiple_of(owner * part, part), part)

    swaps = []
    for turn in range(tp // 2):
        theirs = lines(lax.rem(mate + 2 * turn, tp))
        swaps.append(
            remote(
                mix.at[:, theirs],
                moved.at[:, theirs],
                m_send.at[turn],
                m_recv.at[turn],
                {"tp": mate},
            )
        )
    for one in swaps:
        one.start()
    owners = [lax.rem(me + 2 * turn, tp) for turn in range(1, tp // 2)] + [me]
    outs.wait_recv()
    blocks = pairs + heads
    for one in swaps:
        one.wait_recv()
    near = jnp.concatenate(
        [
            jnp.concatenate([mix[b, lines(owner), :] for b in range(blocks)], axis=1)
            for owner in owners
        ],
        axis=0,
    )
    far = jnp.concatenate(
        [
            jnp.concatenate([moved[b, lines(owner), :] for b in range(blocks)], axis=1)
            for owner in owners
        ],
        axis=0,
    )
    slabs, slab = parts.shape[1], parts.shape[3]
    trades = {}
    for number in range(slabs):
        columns = pl.ds(number * slab, slab)
        result = jnp.dot(near, hw[0, :, columns], preferred_element_type=F32)
        result = result + jnp.dot(far, hw[1, :, columns], preferred_element_type=F32)
        for turn in range(1, tp // 2):
            parts[turn, number] = result[(turn - 1) * part : turn * part].astype(BF16)
            trades[turn, number] = remote(
                parts.at[turn, number],
                got.at[turn, number],
                p_send.at[turn, number],
                p_recv.at[turn, number],
                {"tp": lax.rem(me + 2 * turn, tp)},
            )
            trades[turn, number].start()
        total[:, columns] = result[(tp // 2 - 1) * part :]
    for number in range(slabs):
        columns = pl.ds(number * slab, slab)
        full = total[:, columns]
        for turn in range(1, tp // 2):
            trades[turn, number].wait_recv()
            full = full + got[turn, number].astype(F32)
        total[:, columns] = full
    full = total[...]
    mean = jnp.mean(full * full, axis=-1, keepdims=True)
    out[...] = (full * lax.rsqrt(mean + NORM_EPS) * out_gain[...]).astype(BF16)

    for group_of in (hops, trades):
        for one in group_of.values():
            one.wait_send()
    for one in swaps:
        one.wait_send()
    outs.wait_send()
    for number in range(parts_of):
        for head, condition in own_crosses:
            guarded(condition, crossing(head, place, number).wait_send)
        for head, target, condition in column_goes():
            guarded(condition, column(head, place, target, number).wait_send)
    for stage in relayed:
        for head, source, condition in stage:

            def one(head=head, source=source):
                for number in range(parts_of):
                    crossing(head, 2 * source + lax.rem(place, 2), number).wait_send()

            guarded(condition, one)
    for hop in range(1, sp):
        guarded(place + hop < sp, states[hop].wait_send)
    if moving:
        guarded(late, lambda: [one.wait_send() for one in asks] and None)
        guarded(early, lambda: [one.wait_send() for one in answers] and None)


def per_device(
    sp,
    tp,
    hidden_in,
    in_gain,
    receptance_weight,
    key_weight,
    value_weight,
    decay_down,
    decay_up,
    decay_base,
    decay_shift,
    learn_rate,
    query_pair,
    key_pair,
    value_pair,
    mix_lambda,
    out_recurrent,
    out_attention,
    out_gain,
):
    rows, width = hidden_in.shape
    depth = width * tp
    features = receptance_weight.shape[1]
    heads = mix_lambda.shape[0]
    wide = heads * LANES
    pairs = features // LANES
    low = decay_down.shape[1]
    across = out_recurrent.shape[1]
    part = rows // tp
    count = sp // 2
    movers = max(heads // 2, 1)
    pieces = rows // LANES if rows % LANES == 0 else 1
    slabs = 4 if across % (4 * LANES) == 0 else 1
    shape = jax.ShapeDtypeStruct
    held = pltpu.VMEM

    def paired(weight):
        return weight if heads > 1 else weight.reshape(depth, wide)

    args = (
        hidden_in,
        in_gain.reshape(1, -1),
        receptance_weight,
        key_weight,
        value_weight,
        decay_down,
        decay_up,
        decay_base.reshape(1, -1),
        decay_shift,
        learn_rate.reshape(1, -1),
        paired(query_pair),
        paired(key_pair),
        paired(value_pair),
        mix_lambda,
        out_recurrent,
        out_attention,
        out_gain.reshape(1, -1),
    )
    inside = pl.BlockSpec(memory_space=pltpu.VMEM)
    outside = pl.BlockSpec(memory_space=pl.ANY)
    specs = [inside] * 2 + [outside] * 5 + [inside] * 3 + [outside] * 3
    specs += [pl.BlockSpec(memory_space=pltpu.SMEM)] + [outside] * 2 + [inside]
    raw = (depth, heads, LANES) if heads > 1 else (8, LANES)
    sizes = ((10,), (tp, pieces), (tp, pieces), (1,), (1,))
    sizes += ((heads, count, pieces),) * 4
    sizes += ((sp,), (sp,), (movers,), (movers,), (movers, 2), (movers, 2))
    sizes += ((tp // 2,), (tp // 2,), (tp // 2, slabs), (tp // 2, slabs))
    return tuple(
        pl.pallas_call(
            functools.partial(layer_body, sp, tp),
            out_shape=[shape((part, across), BF16), shape((heads, 2, rows), F32)],
            in_specs=specs,
            out_specs=[inside] * 2,
            scratch_shapes=[
                held((tp, rows, width), BF16),
                held((rows, depth), BF16),
                held((depth, features), BF16),
                held((depth, features), BF16),
                held((depth, features), BF16),
                held((depth, low), BF16),
                held((low, features), BF16),
                held((depth, wide), BF16),
                held((depth, wide), BF16),
                held((depth, wide), BF16),
                held((2, features + wide, across), BF16),
                held(raw, BF16),
                held(raw, BF16),
                held(raw, BF16),
                held((sp, heads, rows, 2 * LANES), BF16),
                held((rows, features), BF16),
                held((rows, features), BF16),
                held((rows, features), BF16),
                held((rows, features), F32),
                held((heads, rows, LANES), BF16),
                held((rows, features), F32),
                held((rows, features), F32),
                held((sp, pairs, 2 * HD, LANES), BF16),
                held((pairs, 2 * LANES, LANES), F32),
                held((2 * rows, LANES), BF16),
                held((2 * rows, 1), F32),
                held((2 * rows, 1), F32),
                held((2 * rows, LANES), F32),
                held((pairs + heads, rows, LANES), BF16),
                held((pairs + heads, rows, LANES), BF16),
                held((movers, rows, LANES), BF16),
                held((movers, rows, LANES), BF16),
                held((movers, 2, rows), F32),
                held((movers, 2, rows), F32),
                held((part, across), F32),
                held((tp // 2, slabs, part, across // slabs), BF16),
                held((tp // 2, slabs, part, across // slabs), BF16),
            ]
            + [pltpu.SemaphoreType.DMA(size) for size in sizes],
            compiler_params=pltpu.CompilerParams(
                collective_id=0, has_side_effects=True, vmem_limit_bytes=62 * 1024 * 1024
            ),
        )(*args)
    )


def solution(mesh):
    in_specs = (
        P("sp", "tp"),
        P(),
        P(None, "tp"),
        P(None, "tp"),
        P(None, "tp"),
        P(),
        P(None, "tp"),
        P("tp"),
        P("sp", "tp"),
        P("tp"),
        P(None, "tp", None),
        P(None, "tp", None),
        P(None, "tp", None),
        P("tp"),
        P("tp", None),
        P("tp", None),
        P(),
    )
    out_specs = (P(("sp", "tp"), None), P("tp", None, "sp"))
    body = functools.partial(per_device, mesh.shape["sp"], mesh.shape["tp"])
    return jax.shard_map(
        body, mesh=mesh, in_specs=in_specs, out_specs=out_specs, check_vma=False
    )
```

time: 97.9 us -> 82.7 us (0.84)
  the two profiles are of different devices: /device:TPU:25 before, /device:TPU:11 now
where the time goes in v1:
time: 82.7 us; the launch traced here: 82.5 us
  Pallas kernels  79.5 us (96%)
  local copies, waits for them, and re-layouts  2.37 us (3%)
    pallas_call x1, Pallas kernels, per_device(): pl.pallas_call(functools.partial(layer_body, sp, tp), out_shape=[shape((p...  79.5 us
    unnamed x4, local copies, waits for them, and re-layouts  2.37 us

profile of v1, /device:TPU:11, one launch (start us, length us, event | category | flops | bytes accessed | tf_op | source)
XLA Modules:
  0.0 82.5 jit_solution(6609105530623472939)
XLA Ops:
  0.6 79.5 %shard_map.176 = (bf16[96,2048]{1,0:T(8,128)(2,1)}, f32[2,2,384]{2,1,0:T(2,128)}) custom-call(bf16[384,512]{1,0:T(8,128)(2,1)} %refs_0_.1, f32[1,2048]{1,0:T(1,128)} %bitcast.4, bf16[2048,256]{1,0:T(8,128)(2,1)} %refs_2_.1, bf16[2048,256]{1,0:T(8,128)(2,1)} %refs_3_.1, bf16[2048,256]{1,0:T(8,128)(2,1)} %refs_4_.1, bf16[2048,128]{1,0:T(8,128)(2,1)} %refs_5_.1, ...), custom_call_target="tpu_custom_call" | custom-call | tf_op jit(solution)/shard_map/pallas_call | solution.py:750
  80.1 0.0 copy-start
  80.1 1.8 %copy.21 = bf16[96,2048]{1,0:T(8,128)(2,1)} copy(bf16[96,2048]{1,0:T(8,128)(2,1)} %get-tuple-element.4) | data formatting | bytes 786432
  81.9 0.0 copy-done
  81.9 0.6 copy.22
Async XLA Ops:
  80.1 1.8 %copy-start = (f32[2,2,384]{2,1,0:T(2,128)S(1)}, f32[2,2,384]{2,1,0:T(2,128)}, u32[]{:S(2)}) copy-start(f32[2,2,384]{2,1,0:T(2,128)} %get-tuple-element.5) | copy-start | bytes 18436

commit v2 on v1

--- a/solution.py
+++ b/solution.py
@@ -128,7 +128,7 @@
         spots = [(turn * group + g, pair) for g in range(group) for pair in range(pairs)]
         items = [local(pair, pl.multiple_of(c * CHUNK, CHUNK)) for c, pair in spots]
         for it in items:
-            scores = dot3(it["left"], it["right"], NT)
+            scores = dot1(it["left"], it["right"], NT)
             it["low"] = jnp.where(strict, scores[:LANES, :LANES], 0.0)
             it["carry"] = jnp.where(strict, scores[:LANES, LANES:], 0.0)
             it["read_erase"] = jnp.where(causal, scores[LANES:, :LANES], 0.0)
@@ -138,28 +138,28 @@
         while size < CHUNK:
             keep = below(size)
             for it in items:
-                it["mid"] = dot3(jnp.where(keep, it["low"], 0.0), it["inv"])
+                it["mid"] = dot1(jnp.where(keep, it["low"], 0.0), it["inv"])
             for it in items:
-                it["inv"] = it["inv"] + dot3(it["inv"], it["mid"])
+                it["inv"] = it["inv"] + dot1(it["inv"], it["mid"])
             size *= 2
         for it in items:
-            it["fed"] = dot3(it["carry"], it["values"])
+            it["fed"] = dot1(it["carry"], it["values"])
         for it in items:
             side = jnp.concatenate([it["against"], it["fed"]], axis=1)
-            it["solved"] = dot3(it["inv"], side)
+            it["solved"] = dot1(it["inv"], side)
         for it in items:
             seen = dot1(it["read_erase"], it["solved"])
             it["heard"] = seen[:, LANES:] + dot1(it["read_keys"], it["values"])
             it["read"] = it["read"] + seen[:, :LANES]
-            it["added"] = dot3(it["values"], it["keys_end"], TN)
+            it["added"] = dot1(it["values"], it["keys_end"], TN)
         for (c, pair), it in zip(spots, items):
             now = state[pair]
             both = jnp.concatenate([it["solved"][:, :LANES], it["read"]], axis=0)
-            met = dot3(both, now, NT)
+            met = dot1(both, now, NT)
             gone = jnp.concatenate(
                 [met[:LANES, :LANES] + it["solved"][:, LANES:], met[:LANES, LANES:]], axis=1
             )
-            later = now * it["whole"] + dot3(gone, it["erase_end"], TN)
+            later = now * it["whole"] + dot1(gone, it["erase_end"], TN)
             state[pair, :LANES, :] = later[:LANES] + it["added"]
             state[pair, LANES:, :] = later[LANES:]
             heard = met[LANES:, :LANES] + it["heard"]
@@ -176,7 +176,39 @@
         end_ref[pair, HD:, :] = (now[LANES : LANES + HD] + now[LANES + HD :]).astype(BF16)
 
 
-def finish_body(out_ref, turn_ref, ends, place, mix_ref):
+def join_body(met, own, following, state):
+    lane = lax.broadcasted_iota(jnp.int32, (1, LANES), 1)
+    first = (lane < HD).astype(F32)
+    second = 1.0 - first
+    line = lax.broadcasted_iota(jnp.int32, (HD, LANES), 0)
+    column = lax.broadcasted_iota(jnp.int32, (HD, LANES), 1)
+    eye = (line == lax.rem(column, HD)).astype(F32)
+
+    def spread(x):
+        return jnp.concatenate([x * first, x * second], axis=0)
+
+    for pair in range(own.shape[0]):
+        both = spread(met[pair, :HD, :].astype(F32))
+        if following is not None:
+            both = jnp.concatenate([both, spread(met[pair, HD:, :].astype(F32))], axis=0)
+
+        def after(block, size):
+            high, low = halves(spread(block[HD : 2 * HD]))
+            moved = dot1(both[:size], high) + dot1(both[:size], low)
+            return [moved[at : at + HD] + moved[at + HD : at + LANES] for at in range(0, size, LANES)]
+
+        later = state[pair, : 2 * HD, :] + jnp.concatenate([jnp.zeros((HD, LANES), F32), eye], axis=0)
+        parts = after(later, 2 * LANES if following is not None else LANES)
+        state[pair, :HD, :] = parts[0] + later[:HD]
+        if following is not None:
+            state[pair, HD : 2 * HD, :] = parts[1] - eye
+        if following is not None:
+            mine = own[pair].astype(F32)
+            parts = after(mine, 2 * LANES)
+            following[pair] = jnp.concatenate([parts[0] + mine[:HD], parts[1]], axis=0).astype(BF16)
+
+
+def finish_body(out_ref, turn_ref, state, mix_ref):
     pairs = out_ref.shape[1] // LANES
     lane = lax.broadcasted_iota(jnp.int32, (1, LANES), 1)
     first = (lane < HD).astype(F32)
@@ -189,12 +221,7 @@
         return jnp.concatenate([x * first, x * second], axis=0)
 
     for pair in range(pairs):
-        entering = jnp.zeros((LANES, LANES), F32)
-        for far, end in ends:
-            block = jnp.where(place >= far, end[pair].astype(F32), 0.0)
-            high, low = halves(entering)
-            move = spread(block[HD:])
-            entering = dot1(high, move) + dot1(low, move) + spread(block[:HD])
+        entering = spread(state[pair, :HD, :])
         columns = pl.ds(pair * LANES, LANES)
         full = out_ref[:, columns] + dot3(turn_ref[:, columns], entering, NT)
 
@@ -208,50 +235,45 @@
         )
 
 
-def update(queries, at, tile, blocks, mask, tops, sums, accs):
-    here = pl.ds(2 * at, 2 * tile)
-    lhs = queries[here, :]
-    scores = [
-        lax.dot_general(lhs, keys, NT, preferred_element_type=F32) for keys, _ in blocks
-    ]
-    if mask is not None:
-        scores = [jnp.where(mask, s, NEGATIVE) for s in scores]
-    old = tops[here, :]
-    top = functools.reduce(jnp.maximum, [jnp.max(s, axis=-1, keepdims=True) for s in scores])
-    top = jnp.maximum(top, old)
-    fade = jnp.exp(old - top)
-    row_sum = sums[here, :] * fade
-    acc = accs[here, :] * fade
-    for s, (_, values) in zip(scores, blocks):
-        weights = jnp.exp(s - top)
-        row_sum = row_sum + jnp.sum(weights, axis=-1, keepdims=True)
-        acc = acc + jnp.dot(weights.astype(BF16), values, preferred_element_type=F32)
-    return here, top, row_sum, acc
-
-
 def attend(q, kv, head, index, lam, queries, tops, sums, accs, mix_ref, log_ref):
-    rows = q.shape[0]
-    tile = LANES if rows % LANES == 0 else rows
-    starts = range(0, rows, tile)
+    tiles = queries.shape[0]
     lane = lax.broadcasted_iota(jnp.int32, (1, LANES), 1)
-    for at in starts:
-        part = q[pl.ds(at, tile), :].astype(F32) * HD ** (-0.5)
-        queries[pl.ds(2 * at, 2 * tile), :] = jnp.concatenate(
+    for tile in range(tiles):
+        part = q[pl.ds(tile * LANES, LANES), :].astype(F32) * HD ** (-0.5)
+        queries[tile] = jnp.concatenate(
             [jnp.where(lane < HD, part, 0.0), jnp.where(lane < HD, 0.0, part)], axis=0
         ).astype(BF16)
     tops[...] = jnp.full(tops.shape, NEGATIVE, F32)
     sums[...] = jnp.zeros(sums.shape, F32)
     accs[...] = jnp.zeros(accs.shape, F32)
 
+    def score(tile, spots, mask):
+        keys = jnp.concatenate([kv[n, head, c, :LANES, :] for n, c in spots], axis=0)
+        s = lax.dot_general(keys, queries[tile], NT, preferred_element_type=F32)
+        return s if mask is None else jnp.where(mask, s, NEGATIVE)
+
+    def absorb(tile, spots, s):
+        values = jnp.concatenate([kv[n, head, c, LANES:, :] for n, c in spots], axis=1)
+        old = tops[tile]
+        top = jnp.maximum(old, jnp.max(s, axis=0, keepdims=True))
+        fade = jnp.exp(old - top)
+        weights = jnp.exp(s - top)
+        row_sum = sums[tile] * fade + jnp.sum(weights, axis=0, keepdims=True)
+        acc = accs[tile] * fade + jnp.dot(
+            values, weights.astype(BF16), preferred_element_type=F32
+        )
+        return top, row_sum, acc
+
     def fold(numbers):
-        blocks = [(kv[n, head, :, :LANES], kv[n, head, :, LANES:]) for n in numbers]
-        for at in starts:
-            here, top, row_sum, acc = update(
-                queries, at, tile, blocks, None, tops, sums, accs
-            )
-            tops[here, :] = top
-            sums[here, :] = row_sum
-            accs[here, :] = acc
+        spots = [(n, c) for n in numbers for c in range(tiles)]
+        scores = {ahead: score(ahead, spots, None) for ahead in range(1)}
+        for tile in range(tiles):
+            if tile + 1 < tiles:
+                scores[tile + 1] = score(tile + 1, spots, None)
+            top, row_sum, acc = absorb(tile, spots, scores.pop(tile))
+            tops[tile] = top
+            sums[tile] = row_sum
+            accs[tile] = acc
 
     def both(turn, carry):
         fold([2 * turn, 2 * turn + 1])
@@ -259,33 +281,36 @@
 
     lax.fori_loop(0, lax.div(index, 2), both, 0)
     pl.when(lax.rem(index, 2) == 1)(lambda: fold([index - 1]))
-    for at in starts:
-        size = at + tile
-        line = lax.broadcasted_iota(jnp.int32, (tile, size), 0) + at
-        seen = line >= lax.broadcasted_iota(jnp.int32, (tile, size), 1)
-        block = (kv[index, head, :size, :LANES], kv[index, head, :size, LANES:])
-        mask = jnp.concatenate([seen, seen], axis=0)
-        _, top, row_sum, acc = update(queries, at, tile, [block], mask, tops, sums, accs)
+    spots = [(index, c) for c in range(tiles)]
+    scores = []
+    for tile in range(tiles):
+        size = (tile + 1) * LANES
+        asking = lax.broadcasted_iota(jnp.int32, (size, LANES), 1) + tile * LANES
+        seen = asking >= lax.broadcasted_iota(jnp.int32, (size, LANES), 0)
+        mask = jnp.concatenate([seen, seen], axis=1)
+        scores.append(score(tile, spots[: tile + 1], mask))
+    results = [absorb(tile, spots[: tile + 1], s) for tile, s in enumerate(scores)]
+    for tile, (top, row_sum, acc) in enumerate(results):
         maps = acc / row_sum
         logs = top + jnp.log(row_sum)
-        flat = jnp.transpose(jnp.broadcast_to(logs, (2 * tile, LANES)))
-        log_ref[0:1, pl.ds(at, tile)] = flat[:1, :tile]
-        log_ref[1:2, pl.ds(at, tile)] = flat[:1, tile:]
-        out = maps[:tile] - lam * maps[tile:]
-        out = out * lax.rsqrt(jnp.mean(out * out, axis=-1, keepdims=True) + HEAD_EPS)
-        mix_ref[pl.ds(at, tile), :] = out.astype(BF16)
+        here = pl.ds(tile * LANES, LANES)
+        log_ref[0:1, here] = logs[:, :LANES]
+        log_ref[1:2, here] = logs[:, LANES:]
+        out = maps[:, :LANES] - lam * maps[:, LANES:]
+        out = out * lax.rsqrt(jnp.mean(out * out, axis=0, keepdims=True) + HEAD_EPS)
+        mix_ref[here, :] = jnp.transpose(out).astype(BF16)
 
 
 def layer_body(sp, tp, *refs):
     (hidden, gain, wr_h, wk_h, wv_h, down_h, up_h, base, shift, learn) = refs[:10]
     (wq_h, wkp_h, wvp_h, lam, rec_h, att_h, out_gain, out, logs) = refs[10:19]
     (xs, normed, wr, wk, wv, down, up, wq, wkp, wvp, hw) = refs[19:30]
-    (wq_p, wkp_p, wvp_p, kv, r, k, v, d, q, heard, turned, ends, state) = refs[30:43]
-    (queries, top, row_sum, acc, mix, moved, q_far, mix_far, log_far) = refs[43:52]
-    (log_got, total, parts, got) = refs[52:56]
-    (load, x_send, x_recv, w_send, w_recv, z_send, z_recv, c_send, c_recv) = refs[56:65]
-    (e_send, e_recv, q_send, q_recv, b_send, b_recv, m_send, m_recv) = refs[65:73]
-    (p_send, p_recv) = refs[73:]
+    (wb, bmix, wq_p, wkp_p, wvp_p, spare, kv, r, k, v, d, q, heard, turned, ends, met, state) = refs[30:47]
+    (queries, top, row_sum, acc, mix, moved, q_far, mix_far, log_far) = refs[47:56]
+    (log_got, total, parts, got) = refs[56:60]
+    (load, x_send, x_recv, w_send, w_recv, z_send, z_recv, c_send, c_recv) = refs[60:69]
+    (e_send, e_recv, q_send, q_recv, b_send, b_recv, m_send, m_recv) = refs[69:77]
+    (p_send, p_recv, g_send, l_send, l_recv) = refs[77:]
     rows, features = r.shape
     heads = q.shape[0]
     wide = heads * LANES
@@ -298,6 +323,7 @@
     mirror = sp - 1 - place
     early = place < count
     late = place >= count
+    stay = (heads - heads // 2) * LANES
     moving = list(range(heads - heads // 2, heads))
     staying = list(range(heads - heads // 2))
     parts_of = z_recv.shape[2]
@@ -308,6 +334,8 @@
         pl.semaphore_signal(barrier, inc=1, device_id={"tp": swapped(me, turn)})
     for hop in range(1, sp):
         pl.semaphore_signal(barrier, inc=1, device_id={"sp": lax.rem(place + hop, sp)})
+    for turn in range(1, tp) if moving else ():
+        pl.semaphore_signal(barrier, inc=1, device_id={"sp": mirror, "tp": swapped(me, turn)})
     pair_loads = heads > 1
     loads = []
     for number, (source, target) in enumerate(
@@ -321,12 +349,13 @@
             (down_h, down),
             (up_h, up),
             (rec_h, hw.at[0, pl.ds(0, features)]),
-            (att_h, hw.at[0, pl.ds(features, wide)]),
-        )
+            (att_h.at[pl.ds(0, stay)], hw.at[0, pl.ds(features, stay)]),
+        )
+        + (((att_h.at[pl.ds(stay, wide - stay)], wb.at[0]),) if moving else ())
     ):
         loads.append(pltpu.make_async_copy(source, target, load.at[number]))
         loads[-1].start()
-    pl.semaphore_wait(barrier, tp - 1 + sp - 1)
+    pl.semaphore_wait(barrier, (2 if moving else 1) * (tp - 1) + sp - 1)
 
     def remote(source, target, send, recv, device):
         return pltpu.make_async_remote_copy(
@@ -351,23 +380,29 @@
         hops[1, number].start()
 
     def unpack(packed, target):
-        def one(turn, carry):
-            lines = pl.ds(pl.multiple_of(turn * 256, 256), 256)
+        lines = target.shape[0]
+        step = lines // 4
+        for turn in range(4):
+            spare[pl.ds(turn * step * heads, step * heads), :] = packed[
+                pl.ds(turn * step * heads, step * heads), :
+            ].astype(F32)
+        for turn in range(4):
             for head in range(heads):
-                target[lines, pl.ds(head * LANES, LANES)] = packed[lines, head, :]
-            return carry
-
-        lax.fori_loop(0, target.shape[0] // 256, one, 0)
-
-    for one in loads[:3]:
-        one.wait()
+                target[pl.ds(turn * step, step), pl.ds(head * LANES, LANES)] = spare[
+                    pl.ds(turn * step * heads + head, step, stride=heads), :
+                ].astype(BF16)
+
+    loads[0].wait()
+    loads[1].wait()
     if pair_loads:
         unpack(wkp_p, wkp)
         unpack(wvp_p, wvp)
+    loads[2].wait()
+    if pair_loads:
         unpack(wq_p, wq)
 
     def column(head, source, target, number):
-        here = kv.at[source, head, chunks[number]]
+        here = kv.at[source, head, number]
         return remote(
             here,
             here,
@@ -380,7 +415,7 @@
         return lax.div(source, 2)
 
     def crossing(head, source, number):
-        here = kv.at[source, head, chunks[number]]
+        here = kv.at[source, head, number]
         return remote(
             here,
             here,
@@ -404,15 +439,13 @@
     ]
     relayed = []
     for far in range(1, count):
-        stage = []
         for head in staying:
-            stage.append((head, level - far, level >= far))
+            relayed.append((head, level - far, level >= far))
         for head in moving:
-            stage.append(
+            relayed.append(
                 (head, level + far, (level < count // 2) & (level + far <= count - 1 - level))
             )
-            stage.append((head, level - far, (level < count // 2) & (level >= far)))
-        relayed.append(stage)
+            relayed.append((head, level - far, (level < count // 2) & (level >= far)))
 
     def guarded(condition, work):
         pl.when(condition)(work)
@@ -426,34 +459,38 @@
                 lambda head=head, target=target: column(head, place, target, number).start(),
             )
 
-    def relay(stage):
-        for head, source, condition in relayed[stage]:
+    def relay(number):
+        for head, source, condition in relayed:
 
             def one(head=head, source=source):
                 slot = 2 * source + lax.rem(place, 2)
-                for number in range(parts_of):
-                    column(head, slot, level, number).wait_recv()
-                    crossing(head, slot, number).start()
+                column(head, slot, level, number).wait_recv()
+                crossing(head, slot, number).start()
 
             guarded(condition, one)
 
     def product(here, weight):
         return jnp.dot(normed[here, :], weight[...], preferred_element_type=F32)
 
-    for number, here in enumerate(chunks):
+    def pass_on(number):
         for turn in range(2, tp, 2):
             hops[turn, number].wait_recv()
             hops[turn + 1, number].start()
+
+    pass_on(0)
+    for number, here in enumerate(chunks):
         for turn in range(1, tp, 2):
             hops[turn, number].wait_recv()
         normalize([hidden] + [xs.at[turn] for turn in range(1, tp)], gain, normed, me, here)
-        keys = product(here, wkp).astype(BF16)
-        values = product(here, wvp).astype(BF16)
+        keys = product(here, wkp)
+        values = product(here, wvp)
         for head in range(heads):
             columns = slice(head * LANES, (head + 1) * LANES)
-            kv[place, head, here, :LANES] = keys[:, columns]
-            kv[place, head, here, LANES:] = values[:, columns]
+            kv[place, head, number, :LANES, :] = keys[:, columns].astype(BF16)
+            kv[place, head, number, LANES:, :] = jnp.transpose(values[:, columns]).astype(BF16)
         send_piece(number)
+        if number + 1 < parts_of:
+            pass_on(number + 1)
         if number == 0:
             for one in loads[3:]:
                 one.wait()
@@ -471,6 +508,20 @@
         pre = jnp.dot(low_rank, up[...], preferred_element_type=F32) + base[...]
         d[here, :] = -DECAY_SCALE * jax.nn.sigmoid(pre) + shift[here, :]
 
+    spreads = {}
+    for turn in range(1, tp) if moving else ():
+        spreads[turn] = remote(
+            wb.at[turn - 1] if turn % 2 else wb.at[0],
+            wb.at[turn],
+            w_send.at[turn],
+            w_recv.at[turn],
+            {"tp": swapped(me, 1 if turn % 2 else turn)},
+        )
+    for turn in range(2, tp, 2) if moving else ():
+        spreads[turn].start()
+    if moving:
+        spreads[1].start()
+
     asks = [
         remote(q.at[head], q_far.at[n], q_send.at[n], q_recv.at[n], {"sp": mirror})
         for n, head in enumerate(moving)
@@ -478,33 +529,53 @@
     if moving:
         guarded(late, lambda: [one.start() for one in asks] and None)
 
-    group = 2 if (rows // CHUNK) % 2 == 0 else 1
+    group = 3 if (rows // CHUNK) % 3 == 0 else 1
     turns = rows // CHUNK // group
     placed = {}
-    for stage in range(count - 1):
-        placed.setdefault(min(stage + 1, turns), []).append(stage)
+    for number in range(parts_of - 1):
+        placed.setdefault(min(number, turns - 1), []).append(number)
 
     def between(turn):
-        for when, stages in placed.items():
-            if when < turns:
-
-                def work(stages=stages):
-                    for stage in stages:
-                        relay(stage)
-
-                pl.when(turn == when)(work)
+        for when, numbers in placed.items():
+
+            def work(numbers=numbers):
+                for number in numbers:
+                    relay(number)
+
+            pl.when(turn == when)(work)
 
     recurrent_body(group, between, r, k, v, d, learn, heard, turned, ends.at[0], state)
-    states = {
-        hop: remote(
-            ends.at[0], ends.at[hop], e_send.at[hop], e_recv.at[hop], {"sp": place + hop}
-        )
-        for hop in range(1, sp)
-    }
-    for hop in range(1, sp):
-        guarded(place + hop < sp, states[hop].start)
-    for stage in placed.get(turns, []):
-        relay(stage)
+    scans = [1 << number for number in range(ends.shape[0])]
+    states = [
+        remote(
+            ends.at[number, :, pl.ds(0, HD if number + 1 == len(scans) else 2 * HD)],
+            met.at[number, :, pl.ds(0, HD if number + 1 == len(scans) else 2 * HD)],
+            e_send.at[number],
+            e_recv.at[number],
+            {"sp": place + hop},
+        )
+        for number, hop in enumerate(scans)
+    ]
+    guarded(place + 1 < sp, states[0].start)
+
+    def scan(number):
+        hop = scans[number]
+        last = number + 1 == len(scans)
+
+        def take():
+            states[number].wait_recv()
+            join_body(met.at[number], ends.at[number], None if last else ends.at[number + 1], state)
+
+        guarded(place >= hop, take)
+        if not last:
+
+            def keep():
+                ends[number + 1] = ends[number]
+
+            guarded(place < hop, keep)
+            guarded(place + 2 * hop < sp, states[number + 1].start)
+
+    relay(parts_of - 1)
 
     def arrive(names, last):
         for source in range(count):
@@ -518,85 +589,59 @@
 
                 guarded((lax.rem(place, 2) != side) & (slot <= last), one)
 
-    answers = []
-    for n, head in enumerate(moving):
-        answers.append(
-            remote(
-                mix_far.at[n],
-                mix.at[pairs + head],
-                b_send.at[n, 0],
-                b_recv.at[n, 0],
-                {"sp": mirror},
+    part = rows // tp
+    mate = swapped(me, 1)
+
+    def lines(owner):
+        return pl.ds(pl.multiple_of(owner * part, part), part)
+
+    answers, gives, tells = [], [], []
+    if moving:
+        for turn in range(tp):
+            owner = swapped(me, turn)
+            answers.append(
+                remote(
+                    mix_far.at[:, lines(owner)],
+                    bmix.at[turn],
+                    b_send.at[turn],
+                    b_recv.at[turn],
+                    {"sp": mirror, "tp": owner} if turn else {"sp": mirror},
+                )
             )
-        )
-        answers.append(
-            remote(
-                log_far.at[n], log_got.at[n], b_send.at[n, 1], b_recv.at[n, 1], {"sp": mirror}
-            )
+            if turn:
+                gives.append(
+                    remote(
+                        mix.at[pl.ds(pairs + moving[0], len(moving)), lines(owner)],
+                        bmix.at[turn],
+                        g_send.at[turn],
+                        b_recv.at[turn],
+                        {"tp": owner},
+                    )
+                )
+        tells.append(
+            remote(log_far, log_got, l_send.at[0], l_recv.at[0], {"sp": mirror})
         )
     work = (queries, top, row_sum, acc)
 
-    if moving:
-
-        def foreign():
-            arrive(moving, mirror)
-            for n, head in enumerate(moving):
-                asks[n].wait_recv()
-                attend(
-                    q_far.at[n], kv, head, mirror, lam[head], *work, mix_far.at[n], log_far.at[n]
-                )
-                answers[2 * n].start()
-                answers[2 * n + 1].start()
-
-        guarded(early, foreign)
+    state[...] = jnp.zeros(state.shape, F32)
+    scan(0)
     arrive(staying, place)
     for head in staying:
         attend(
             q.at[head], kv, head, place, lam[head], *work, mix.at[pairs + head], logs.at[head]
         )
-    if moving:
-
-        def local():
-            for head in moving:
-                attend(
-                    q.at[head],
-                    kv,
-                    head,
-                    place,
-                    lam[head],
-                    *work,
-                    mix.at[pairs + head],
-                    logs.at[head],
-                )
-
-        guarded(early, local)
-    for hop in range(1, sp):
-        guarded(place >= hop, states[hop].wait_recv)
-    finish_body(
-        heard, turned, [(hop, ends.at[hop]) for hop in range(sp - 1, 0, -1)], place, mix
-    )
-    if moving:
-
-        def collect():
-            for one in answers:
-                one.wait_recv()
-            for n, head in enumerate(moving):
-                logs[head] = log_got[n]
-
-        guarded(late, collect)
-
-    part = rows // tp
-    mate = swapped(me, 1)
-
-    def lines(owner):
-        return pl.ds(pl.multiple_of(owner * part, part), part)
-
+    for number in range(1, len(scans) - 1):
+        scan(number)
+    if len(scans) > 1:
+        scan(len(scans) - 1)
+    finish_body(heard, turned, state, mix)
+    blocks = pairs + len(staying)
     swaps = []
     for turn in range(tp // 2):
         theirs = lines(lax.rem(mate + 2 * turn, tp))
         swaps.append(
             remote(
-                mix.at[:, theirs],
+                mix.at[pl.ds(0, blocks), theirs],
                 moved.at[:, theirs],
                 m_send.at[turn],
                 m_recv.at[turn],
@@ -607,7 +652,6 @@
         one.start()
     owners = [lax.rem(me + 2 * turn, tp) for turn in range(1, tp // 2)] + [me]
     outs.wait_recv()
-    blocks = pairs + heads
     for one in swaps:
         one.wait_recv()
     near = jnp.concatenate(
@@ -641,9 +685,65 @@
             )
             trades[turn, number].start()
         total[:, columns] = result[(tp // 2 - 1) * part :]
+    if moving:
+        spreads[1].wait_recv()
+        for turn in range(2, tp, 2):
+            spreads[turn].wait_recv()
+            spreads[turn + 1].start()
+    if moving:
+
+        def foreign():
+            arrive(moving, mirror)
+            for n, head in enumerate(moving):
+                asks[n].wait_recv()
+                attend(
+                    q_far.at[n], kv, head, mirror, lam[head], *work, mix_far.at[n], log_far.at[n]
+                )
+            for one in answers + tells:
+                one.start()
+
+        guarded(early, foreign)
+    if moving:
+
+        def local():
+            for head in moving:
+                attend(
+                    q.at[head],
+                    kv,
+                    head,
+                    place,
+                    lam[head],
+                    *work,
+                    mix.at[pairs + head],
+                    logs.at[head],
+                )
+            for one in gives:
+                one.start()
+            for n, head in enumerate(moving):
+                bmix[0, n] = mix[pairs + head, lines(me), :]
+            for one in gives:
+                one.wait_recv()
+
+        def collect():
+            for one in answers + tells:
+                one.wait_recv()
+            for n, head in enumerate(moving):
+                logs[head] = log_got[n]
+
+        guarded(early, local)
+        guarded(late, collect)
+    if moving:
+        for turn in range(3, tp, 2):
+            spreads[turn].wait_recv()
+        beside = jnp.concatenate(
+            [bmix[turn, n] for turn in range(tp) for n in range(len(moving))], axis=1
+        )
     for number in range(slabs):
         columns = pl.ds(number * slab, slab)
         full = total[:, columns]
+        if moving:
+            weights = jnp.concatenate([wb[turn, :, columns] for turn in range(tp)], axis=0)
+            full = full + jnp.dot(beside, weights, preferred_element_type=F32)
         for turn in range(1, tp // 2):
             trades[turn, number].wait_recv()
             full = full + got[turn, number].astype(F32)
@@ -652,7 +752,7 @@
     mean = jnp.mean(full * full, axis=-1, keepdims=True)
     out[...] = (full * lax.rsqrt(mean + NORM_EPS) * out_gain[...]).astype(BF16)
 
-    for group_of in (hops, trades):
+    for group_of in (hops, trades, spreads):
         for one in group_of.values():
             one.wait_send()
     for one in swaps:
@@ -663,19 +763,19 @@
             guarded(condition, crossing(head, place, number).wait_send)
         for head, target, condition in column_goes():
             guarded(condition, column(head, place, target, number).wait_send)
-    for stage in relayed:
-        for head, source, condition in stage:
-
-            def one(head=head, source=source):
-                for number in range(parts_of):
-                    crossing(head, 2 * source + lax.rem(place, 2), number).wait_send()
-
-            guarded(condition, one)
-    for hop in range(1, sp):
-        guarded(place + hop < sp, states[hop].wait_send)
+    for head, source, condition in relayed:
+
+        def one(head=head, source=source):
+            for number in range(parts_of):
+                slot = 2 * source + lax.rem(place, 2)
+                crossing(head, slot, number).wait_send()
+
+        guarded(condition, one)
+    for number, hop in enumerate(scans):
+        guarded(place + hop < sp, states[number].wait_send)
     if moving:
         guarded(late, lambda: [one.wait_send() for one in asks] and None)
-        guarded(early, lambda: [one.wait_send() for one in answers] and None)
+        guarded(early, lambda: [one.wait_send() for one in answers + gives + tells] and None)
 
 
 def per_device(
@@ -710,13 +810,15 @@
     part = rows // tp
     count = sp // 2
     movers = max(heads // 2, 1)
-    pieces = rows // LANES if rows % LANES == 0 else 1
+    stay = (heads - heads // 2) * LANES
+    gone = max(wide - stay, 16)
+    pieces = rows // LANES
     slabs = 4 if across % (4 * LANES) == 0 else 1
     shape = jax.ShapeDtypeStruct
     held = pltpu.VMEM
 
     def paired(weight):
-        return weight if heads > 1 else weight.reshape(depth, wide)
+        return weight.reshape(depth * heads, LANES)
 
     args = (
         hidden_in,
@@ -741,11 +843,13 @@
     outside = pl.BlockSpec(memory_space=pl.ANY)
     specs = [inside] * 2 + [outside] * 5 + [inside] * 3 + [outside] * 3
     specs += [pl.BlockSpec(memory_space=pltpu.SMEM)] + [outside] * 2 + [inside]
-    raw = (depth, heads, LANES) if heads > 1 else (8, LANES)
-    sizes = ((10,), (tp, pieces), (tp, pieces), (1,), (1,))
+    raw = (depth * heads, LANES) if heads > 1 else (16, LANES)
+    scans = max((sp - 1).bit_length(), 1)
+    sizes = ((11,), (tp, pieces), (tp, pieces), (tp,), (tp,))
     sizes += ((heads, count, pieces),) * 4
-    sizes += ((sp,), (sp,), (movers,), (movers,), (movers, 2), (movers, 2))
+    sizes += ((scans,), (scans,), (movers,), (movers,), (tp,), (tp,))
     sizes += ((tp // 2,), (tp // 2,), (tp // 2, slabs), (tp // 2, slabs))
+    sizes += ((tp,), (1,), (1,))
     return tuple(
         pl.pallas_call(
             functools.partial(layer_body, sp, tp),
@@ -763,11 +867,14 @@
                 held((depth, wide), BF16),
                 held((depth, wide), BF16),
                 held((depth, wide), BF16),
-                held((2, features + wide, across), BF16),
+                held((2, features + stay, across), BF16),
+                held((tp, gone, across), BF16),
+                held((tp, movers, part, LANES), BF16),
                 held(raw, BF16),
                 held(raw, BF16),
                 held(raw, BF16),
-                held((sp, heads, rows, 2 * LANES), BF16),
+                held(raw, F32),
+                held((sp, heads, pieces, 2 * LANES, LANES), BF16),
                 held((rows, features), BF16),
                 held((rows, features), BF16),
                 held((rows, features), BF16),
@@ -775,14 +882,15 @@
                 held((heads, rows, LANES), BF16),
                 held((rows, features), F32),
                 held((rows, features), F32),
-                held((sp, pairs, 2 * HD, LANES), BF16),
+                held((scans, pairs, 2 * HD, LANES), BF16),
+                held((scans, pairs, 2 * HD, LANES), BF16),
                 held((pairs, 2 * LANES, LANES), F32),
-                held((2 * rows, LANES), BF16),
-                held((2 * rows, 1), F32),
-                held((2 * rows, 1), F32),
-                held((2 * rows, LANES), F32),
+                held((pieces, 2 * LANES, LANES), BF16),
+                held((pieces, 1, 2 * LANES), F32),
+                held((pieces, 1, 2 * LANES), F32),
+                held((pieces, LANES, 2 * LANES), F32),
                 held((pairs + heads, rows, LANES), BF16),
-                held((pairs + heads, rows, LANES), BF16),
+                held((pairs + heads - heads // 2, rows, LANES), BF16),
                 held((movers, rows, LANES), BF16),
                 held((movers, rows, LANES), BF16),
                 held((movers, 2, rows), F32),

time: 82.7 us -> 60.7 us (0.73)
  Pallas kernels: 79.5 us -> 57 us
    pallas_call x1, Pallas kernels: 79.5 us -> 57 us  [per_device(): pl.pallas_call(functools.partial(layer_body, sp, tp), out_shape=[shape((p...]
where the time goes in v2:
time: 60.7 us; the launch traced here: 60 us
  Pallas kernels  57 us (94%)
  local copies, waits for them, and re-layouts  2.37 us (4%)
  between operations  0.65 us (1%)
    pallas_call x1, Pallas kernels, per_device(): pl.pallas_call(functools.partial(layer_body, sp, tp), out_shape=[shape((p...  57 us
    unnamed x4, local copies, waits for them, and re-layouts  2.37 us

profile of v2, /device:TPU:11, one launch (start us, length us, event | category | flops | bytes accessed | tf_op | source)
XLA Modules:
  0.0 60.0 jit_solution(16132616698897131126)
XLA Ops:
  0.6 57.0 %shard_map.176 = (bf16[96,2048]{1,0:T(8,128)(2,1)}, f32[2,2,384]{2,1,0:T(2,128)}) custom-call(bf16[384,512]{1,0:T(8,128)(2,1)} %refs_0_.1, f32[1,2048]{1,0:T(1,128)} %bitcast.10, bf16[2048,256]{1,0:T(8,128)(2,1)} %refs_2_.1, bf16[2048,256]{1,0:T(8,128)(2,1)} %refs_3_.1, bf16[2048,256]{1,0:T(8,128)(2,1)} %refs_4_.1, bf16[2048,128]{1,0:T(8,128)(2,1)} %refs_5_.1, ...), custom_call_target="tpu_custom_call" | custom-call | tf_op jit(solution)/shard_map/pallas_call | solution.py:854
  57.6 0.0 copy-start
  57.6 1.8 %copy.21 = bf16[96,2048]{1,0:T(8,128)(2,1)} copy(bf16[96,2048]{1,0:T(8,128)(2,1)} %get-tuple-element.4) | data formatting | bytes 786432
  59.4 0.0 copy-done
  59.4 0.6 copy.22
Async XLA Ops:
  57.6 1.8 %copy-start = (f32[2,2,384]{2,1,0:T(2,128)S(1)}, f32[2,2,384]{2,1,0:T(2,128)}, u32[]{:S(2)}) copy-start(f32[2,2,384]{2,1,0:T(2,128)} %get-tuple-element.5) | copy-start | bytes 18436

commit v3 on v2

--- a/solution.py
+++ b/solution.py
@@ -301,6 +301,17 @@
         mix_ref[here, :] = jnp.transpose(out).astype(BF16)
 
 
+def settle_body(first, second, out, logs, done):
+    moves = [
+        pltpu.make_async_copy(first, out, done.at[0]),
+        pltpu.make_async_copy(second, logs, done.at[1]),
+    ]
+    for one in moves:
+        one.start()
+    for one in moves:
+        one.wait()
+
+
 def layer_body(sp, tp, *refs):
     (hidden, gain, wr_h, wk_h, wv_h, down_h, up_h, base, shift, learn) = refs[:10]
     (wq_h, wkp_h, wvp_h, lam, rec_h, att_h, out_gain, out, logs) = refs[10:19]
@@ -459,7 +470,7 @@
                 lambda head=head, target=target: column(head, place, target, number).start(),
             )
 
-    def relay(number):
+    def relay(number, also=None):
         for head, source, condition in relayed:
 
             def one(head=head, source=source):
@@ -467,7 +478,7 @@
                 column(head, slot, level, number).wait_recv()
                 crossing(head, slot, number).start()
 
-            guarded(condition, one)
+            guarded(condition if also is None else condition & also, one)
 
     def product(here, weight):
         return jnp.dot(normed[here, :], weight[...], preferred_element_type=F32)
@@ -532,6 +543,7 @@
     group = 3 if (rows // CHUNK) % 3 == 0 else 1
     turns = rows // CHUNK // group
     placed = {}
+    highest = level == count - 1
     for number in range(parts_of - 1):
         placed.setdefault(min(number, turns - 1), []).append(number)
 
@@ -540,7 +552,7 @@
 
             def work(numbers=numbers):
                 for number in numbers:
-                    relay(number)
+                    relay(number, highest if number else None)
 
             pl.when(turn == when)(work)
 
@@ -575,6 +587,8 @@
             guarded(place < hop, keep)
             guarded(place + 2 * hop < sp, states[number + 1].start)
 
+    for number in range(1, parts_of - 1):
+        relay(number, level < count - 1)
     relay(parts_of - 1)
 
     def arrive(names, last):
@@ -625,16 +639,19 @@
 
     state[...] = jnp.zeros(state.shape, F32)
     scan(0)
+    for number in range(1, len(scans) - 1):
+        guarded(early, lambda number=number: scan(number))
+    pl.when(early)(lambda: finish_body(heard, turned, state, mix))
     arrive(staying, place)
     for head in staying:
         attend(
             q.at[head], kv, head, place, lam[head], *work, mix.at[pairs + head], logs.at[head]
         )
     for number in range(1, len(scans) - 1):
-        scan(number)
+        guarded(late, lambda number=number: scan(number))
     if len(scans) > 1:
         scan(len(scans) - 1)
-    finish_body(heard, turned, state, mix)
+    pl.when(late)(lambda: finish_body(heard, turned, state, mix))
     blocks = pairs + len(staying)
     swaps = []
     for turn in range(tp // 2):
@@ -651,9 +668,6 @@
     for one in swaps:
         one.start()
     owners = [lax.rem(me + 2 * turn, tp) for turn in range(1, tp // 2)] + [me]
-    outs.wait_recv()
-    for one in swaps:
-        one.wait_recv()
     near = jnp.concatenate(
         [
             jnp.concatenate([mix[b, lines(owner), :] for b in range(blocks)], axis=1)
@@ -661,6 +675,14 @@
         ],
         axis=0,
     )
+    slabs, slab = parts.shape[1], parts.shape[3]
+    begun = [
+        jnp.dot(near, hw[0, :, pl.ds(number * slab, slab)], preferred_element_type=F32)
+        for number in range(slabs)
+    ]
+    outs.wait_recv()
+    for one in swaps:
+        one.wait_recv()
     far = jnp.concatenate(
         [
             jnp.concatenate([moved[b, lines(owner), :] for b in range(blocks)], axis=1)
@@ -668,12 +690,12 @@
         ],
         axis=0,
     )
-    slabs, slab = parts.shape[1], parts.shape[3]
     trades = {}
     for number in range(slabs):
         columns = pl.ds(number * slab, slab)
-        result = jnp.dot(near, hw[0, :, columns], preferred_element_type=F32)
-        result = result + jnp.dot(far, hw[1, :, columns], preferred_element_type=F32)
+        result = begun[number] + jnp.dot(
+            far, hw[1, :, columns], preferred_element_type=F32
+        )
         for turn in range(1, tp // 2):
             parts[turn, number] = result[(turn - 1) * part : turn * part].astype(BF16)
             trades[turn, number] = remote(
@@ -850,10 +872,10 @@
     sizes += ((scans,), (scans,), (movers,), (movers,), (tp,), (tp,))
     sizes += ((tp // 2,), (tp // 2,), (tp // 2, slabs), (tp // 2, slabs))
     sizes += ((tp,), (1,), (1,))
-    return tuple(
+    made = tuple(
         pl.pallas_call(
             functools.partial(layer_body, sp, tp),
-            out_shape=[shape((part, across), BF16), shape((heads, 2, rows), F32)],
+            out_shape=[pltpu.VMEM((part, across), BF16), pltpu.VMEM((heads, 2, rows), F32)],
             in_specs=specs,
             out_specs=[inside] * 2,
             scratch_shapes=[
@@ -905,6 +927,16 @@
             ),
         )(*args)
     )
+    return tuple(
+        pl.pallas_call(
+            settle_body,
+            out_shape=[shape((part, across), BF16), shape((heads, 2, rows), F32)],
+            in_specs=[outside] * 2,
+            out_specs=[outside] * 2,
+            scratch_shapes=[pltpu.SemaphoreType.DMA((2,))],
+            compiler_params=pltpu.CompilerParams(vmem_limit_bytes=1024 * 1024),
+        )(*made)
+    )
 
 
 def solution(mesh):

time: 60.7 us -> 57.4 us (0.946)
  local copies, waits for them, and re-layouts: 2.37 us -> 0 us
  Pallas kernels: 57 us -> 56.1 us
    unnamed x4 -> x0, local copies, waits for them, and re-layouts: 2.37 us -> none
    pallas_call x1 -> x2, Pallas kernels: 57 us -> 56.1 us  [the longest x1 55.4 us: per_device(): pl.pallas_call(functools.partial(layer_body, sp, tp), out_shape=[pltpu.VM...]
where the time goes in v3:
time: 57.4 us; the launch traced here: 56.9 us
  Pallas kernels  56.1 us (98%)
  between operations  0.81 us (1%)
    pallas_call x1, Pallas kernels, per_device(): pl.pallas_call(functools.partial(layer_body, sp, tp), out_shape=[pltpu.VM...  55.4 us

profile of v3, /device:TPU:11, one launch (start us, length us, event | category | flops | bytes accessed | tf_op | source)
XLA Modules:
  0.0 56.9 jit_solution(12795462472391639247)
XLA Ops:
  0.6 55.4 %shard_map.176 = (bf16[96,2048]{1,0:T(8,128)(2,1)S(1)}, f32[2,2,384]{2,1,0:T(2,128)S(1)}) custom-call(bf16[384,512]{1,0:T(8,128)(2,1)} %refs_0_.1, f32[1,2048]{1,0:T(1,128)} %bitcast.10, bf16[2048,256]{1,0:T(8,128)(2,1)} %refs_2_.1, bf16[2048,256]{1,0:T(8,128)(2,1)} %refs_3_.1, bf16[2048,256]{1,0:T(8,128)(2,1)} %refs_4_.1, bf16[2048,128]{1,0:T(8,128)(2,1)} %refs_5_.1, ...), custom_call_target="tpu_custom_call" | custom-call | tf_op jit(solution)/shard_map/pallas_call | solution.py:876
  56.0 0.8 %shard_map.177 = (bf16[96,2048]{1,0:T(8,128)(2,1)}, f32[2,2,384]{2,1,0:T(2,128)}) custom-call(bf16[96,2048]{1,0:T(8,128)(2,1)S(1)} %get-tuple-element.4.first, f32[2,2,384]{2,1,0:T(2,128)S(1)} %get-tuple-element.5.second), custom_call_target="tpu_custom_call" | custom-call | tf_op jit(solution)/shard_map/pallas_call | solution.py:931
